TPU v7x, 32 devices: a whole 2x2x4 slice. The times are simulated.
32 devices in a mesh: sp: 4 (over z), fs: 4 (over y, x), tp: 2 (over core).
Axes of the slice: x: 2, y: 2, z: 4, core: 2. Of those that a mesh axis runs over, the one named last changes fastest.
Arguments:
- statespace_input: bfloat16 [4, 1536, 2048], P('fs', 'sp', 'tp'), may hold values from -6 to 6
- output_gate_input: bfloat16 [4, 1536, 2048], P('fs', 'sp', 'tp'), may hold values from -6 to 6
- state_input_projection: bfloat16 [4, 1536, 512], P('fs', 'sp', 'tp'), may hold values from -6 to 6
- state_output_projection: bfloat16 [4, 1536, 512], P('fs', 'sp', 'tp'), may hold values from -6 to 6
- step_size_input: bfloat16 [4, 1536, 32], P('fs', 'sp', 'tp'), may hold values from -5 to 5
- added_log_decay: float32 [4, 1536, 32], P('fs', 'sp', 'tp'), may hold values from -0.7 to 0
- logarithm_rates: float32 [32], replicated, may hold values from -20 to -2.9
- head_channel_taps: bfloat16 [4, 2048], replicated, may hold values from -3 to 3
- input_projection_taps: bfloat16 [4, 512], replicated, may hold values from -3 to 3
- output_projection_taps: bfloat16 [4, 512], replicated, may hold values from -3 to 3
- input_projection_bias: bfloat16 [512], replicated, may hold values from -0.59765625 to -0.19921875
- group_norm_gain: bfloat16 [2048], replicated, may hold values from 0.099609375 to 1.8984375
- pooling_input: bfloat16 [4, 1536, 1024], P('fs', 'sp', 'tp'), may hold values from -6 to 6
- pooling_group_weight: bfloat16 [4, 256, 256], replicated, may hold values from -0.375 to 0.375
- pooling_channel_scale: bfloat16 [1024], replicated, may hold values from 0.099609375 to 1.8984375
- statespace_output_weight: bfloat16 [2048, 4096], P('tp', ('sp', 'fs')), may hold values from -8 to 8
- pooling_output_weight: bfloat16 [1024, 4096], P('tp', ('sp', 'fs')), may hold values from -8 to 8
- output_norm_gain: bfloat16 [4096], replicated, may hold values from 0.099609375 to 1.8984375
Outputs:
- output: bfloat16 [4, 1536, 4096], P('fs', 'sp', 'tp')
All inputs are finite; a program needn't handle non-finite values.
Results may differ from a plain program's by a relative error of at most 0.02.
Values may be sent and summed in bfloat16 or wider, within the bound.
A program may use at most 128 MiB of HBM per device.

v0:
```python
import jax
import jax.numpy as jnp
from jax import lax
from jax.sharding import PartitionSpec as P

D = 4096
HEAD_DIM = 64
STATE = 128
CONV = 4
BLOCK = 128
POOL_GROUPS = 4
POOL_GROUP = 256


eps = 1e-06


def passed_along(block, axis, distance):
    devices = range(lax.axis_size(axis))
    route = [(i - distance, i) for i in devices if i - distance in devices]
    return lax.ppermute(block, axis, route)


def entering_2(array, axis, join, neutral):
    place = lax.axis_index(axis)
    gathered = jax.tree.map(
        lambda a, kind: lax.all_gather(a.astype(kind), axis), array, (jnp.bfloat16, jnp.bfloat16)
    )
    state = jax.tree.map(lambda a, e: jnp.zeros_like(a) + jnp.asarray(e, a.dtype), array, neutral)

    def one(lap, state):
        return join(
            state,
            jax.tree.map(
                lambda a, own: lax.dynamic_index_in_dim(a, lap, 0, False).astype(own.dtype),
                gathered,
                array,
            ),
        )

    return lax.fori_loop(0, place, one, state)


def causal_taps(input_rows, prior_rows, tap_weights, offset_bias):
    padded = jnp.concatenate([prior_rows, input_rows], axis=0).astype(jnp.float32)
    tok_rows = input_rows.shape[0]
    running = jnp.zeros(input_rows.shape, jnp.float32) + offset_bias
    for tap_index in range(tap_weights.shape[0]):
        running = (
            running
            + tap_weights[tap_index].astype(jnp.float32) * padded[tap_index : tap_index + tok_rows]
        )
    return jax.nn.silu(running).astype(jnp.bfloat16)


def pool_mix(input_rows, prior_rows, positions, group_ids, local_weight, local_scale):
    tail_rows = prior_rows.shape[0]
    tok_rows = input_rows.shape[0]
    padded = jnp.concatenate([prior_rows, input_rows], axis=0).astype(jnp.float32)
    window_reach = jnp.left_shift(jnp.int32(2), group_ids)
    running = jnp.zeros(input_rows.shape, jnp.float32)
    for offset_back in range(tail_rows + 1):
        start_row = tail_rows - offset_back
        running = running + padded[start_row : start_row + tok_rows] * (
            offset_back < window_reach
        ).astype(jnp.float32)
    window_count = jnp.minimum(positions[:, None] + 1.0, window_reach.astype(jnp.float32)[None, :])
    pooled = (running / window_count - input_rows.astype(jnp.float32)).astype(jnp.bfloat16)
    grouped = pooled.reshape(tok_rows, local_weight.shape[0], local_weight.shape[1])
    mixed = jnp.einsum("lgc,gcd->lgd", grouped, local_weight, preferred_element_type=jnp.float32)
    return (mixed.reshape(input_rows.shape) * local_scale.astype(jnp.float32)).astype(jnp.bfloat16)


def join_states(earlier, later_part):
    return (
        earlier[0] + later_part[0],
        earlier[1] * jnp.exp(later_part[0])[..., None, None] + later_part[1],
    )


def body(
    statespace_input,
    output_gate_input,
    state_input_projection,
    state_output_projection,
    step_size_input,
    added_log_decay,
    logarithm_rates,
    head_channel_taps,
    input_projection_taps,
    output_projection_taps,
    input_projection_bias,
    group_norm_gain,
    pooling_input,
    pooling_group_weight,
    pooling_channel_scale,
    statespace_output_weight,
    pooling_output_weight,
    output_norm_gain,
):
    core_index = lax.axis_index("tp")
    core_count = lax.axis_size("tp")
    seq_index = lax.axis_index("sp")
    head_channel_rows = statespace_input[0]
    output_gate_rows = output_gate_input[0]
    input_projection_rows = state_input_projection[0]
    output_projection_rows = state_output_projection[0]
    step_size_rows = step_size_input[0]
    decay_spikes = added_log_decay[0]
    pooling_rows = pooling_input[0]
    tok_rows = head_channel_rows.shape[0]
    inner_local = head_channel_rows.shape[1]
    heads_local = step_size_rows.shape[1]
    state_local = input_projection_rows.shape[1]
    pool_local = pooling_rows.shape[1]
    groups_local = state_local // STATE
    per_group = heads_local // groups_local
    groups_pool = pool_local // POOL_GROUP
    pool_tail = 2**POOL_GROUPS - 1
    conv_tail = CONV - 1
    prior_x, prior_b, prior_c, prior_pool = passed_along(
        (
            head_channel_rows[tok_rows - conv_tail :],
            input_projection_rows[tok_rows - conv_tail :],
            output_projection_rows[tok_rows - conv_tail :],
            pooling_rows[tok_rows - pool_tail :],
        ),
        "sp",
        1,
    )
    taps_x = lax.dynamic_slice_in_dim(head_channel_taps, core_index * inner_local, inner_local, 1)
    taps_b = lax.dynamic_slice_in_dim(
        input_projection_taps, core_index * state_local, state_local, 1
    )
    taps_c = lax.dynamic_slice_in_dim(
        output_projection_taps, core_index * state_local, state_local, 1
    )
    bias_b = lax.dynamic_slice_in_dim(
        input_projection_bias, core_index * state_local, state_local, 0
    )
    gain_ssd = lax.dynamic_slice_in_dim(group_norm_gain, core_index * inner_local, inner_local, 0)
    head_decay_rates = jnp.exp(
        lax.dynamic_slice_in_dim(logarithm_rates, core_index * heads_local, heads_local, 0)
    )
    gain_pool = lax.dynamic_slice_in_dim(
        pooling_channel_scale, core_index * pool_local, pool_local, 0
    )
    weight_pool = lax.dynamic_slice_in_dim(
        pooling_group_weight, core_index * groups_pool, groups_pool, 0
    )
    x_conv = causal_taps(head_channel_rows, prior_x, taps_x, 0.0)
    b_conv = causal_taps(input_projection_rows, prior_b, taps_b, bias_b.astype(jnp.float32))
    c_conv = causal_taps(output_projection_rows, prior_c, taps_c, 0.0)
    blocks = tok_rows // BLOCK
    discrete_step_size = jax.nn.softplus(step_size_rows.astype(jnp.float32))
    logarithm_decay = -discrete_step_size * head_decay_rates + decay_spikes
    cumulative_decay = jnp.cumsum(
        logarithm_decay.reshape(blocks, BLOCK, groups_local, per_group), axis=1
    )
    cum_t = cumulative_decay.transpose(0, 2, 3, 1)
    step_t = discrete_step_size.reshape(blocks, BLOCK, groups_local, per_group).transpose(
        0, 2, 3, 1
    )
    heads_x = x_conv.reshape(blocks, BLOCK, groups_local, per_group, HEAD_DIM)
    group_b = b_conv.reshape(blocks, BLOCK, groups_local, STATE)
    group_c = c_conv.reshape(blocks, BLOCK, groups_local, STATE)
    scores = jnp.einsum("ktgn,kugn->kgtu", group_c, group_b, preferred_element_type=jnp.float32)
    causal = jnp.arange(BLOCK)[:, None] >= jnp.arange(BLOCK)[None, :]
    decay_gap = cum_t[..., :, None] - cum_t[..., None, :]
    decay_factor = jnp.where(causal, jnp.exp(jnp.where(causal, decay_gap, 0.0)), 0.0)
    weights = (scores[:, :, None] * decay_factor * step_t[..., None, :]).astype(jnp.bfloat16)
    within = jnp.einsum("kgetu,kugep->ktgep", weights, heads_x, preferred_element_type=jnp.float32)
    block_end = cum_t[..., -1]
    end_weight = jnp.exp(block_end[..., None] - cum_t) * step_t
    scaled_x = (heads_x * end_weight.transpose(0, 3, 1, 2)[..., None]).astype(jnp.bfloat16)
    block_state = jnp.einsum(
        "kugep,kugn->kgepn", scaled_x, group_b, preferred_element_type=jnp.float32
    )

    def local_chain(state_now, current_inputs):
        piece_state, piece_fall = current_inputs
        return (state_now * jnp.exp(piece_fall)[..., None, None] + piece_state, state_now)

    final_state, local_entering = lax.scan(
        local_chain, jnp.zeros(block_state.shape[1:], jnp.float32), (block_state, block_end)
    )
    log_total = jnp.sum(block_end, axis=0)
    prefix_log = jnp.cumsum(block_end, axis=0) - block_end
    log_before, state_before = entering_2(
        (log_total, final_state),
        "sp",
        join_states,
        (jnp.zeros_like(log_total), jnp.zeros_like(final_state)),
    )
    entering = (local_entering + jnp.exp(prefix_log)[..., None, None] * state_before[None]).astype(
        jnp.bfloat16
    )
    carried_out = jnp.einsum(
        "ktgn,kgepn->ktgep", group_c, entering, preferred_element_type=jnp.float32
    )
    carried_out = carried_out * jnp.exp(cumulative_decay)[..., None]
    mixed_ssd = (within + carried_out).reshape(tok_rows, inner_local) * jax.nn.silu(
        output_gate_rows.astype(jnp.float32)
    )
    grouped = mixed_ssd.reshape(tok_rows, groups_local, inner_local // groups_local)
    normed = grouped * lax.rsqrt(jnp.mean(grouped * grouped, axis=-1, keepdims=True) + eps)
    ssd_out = (normed.reshape(tok_rows, inner_local) * gain_ssd.astype(jnp.float32)).astype(
        jnp.bfloat16
    )
    positions = (seq_index * tok_rows + jnp.arange(tok_rows, dtype=jnp.int32)).astype(jnp.float32)
    group_ids = core_index * groups_pool + jnp.arange(pool_local, dtype=jnp.int32) // POOL_GROUP
    pool_out = pool_mix(pooling_rows, prior_pool, positions, group_ids, weight_pool, gain_pool)
    half_width = D // core_count
    gain_out = lax.dynamic_slice_in_dim(
        output_norm_gain, core_index * half_width, half_width, 0
    ).astype(jnp.float32)
    whole_ssd, whole_pool = (
        lax.all_gather(statespace_output_weight, ("sp", "fs"), axis=1, tiled=True),
        lax.all_gather(pooling_output_weight, ("sp", "fs"), axis=1, tiled=True),
    )
    rows_ssd, rows_pool = (
        lax.all_to_all(whole_ssd, "tp", split_axis=1, concat_axis=0, tiled=True),
        lax.all_to_all(whole_pool, "tp", split_axis=1, concat_axis=0, tiled=True),
    )
    every_ssd, every_pool = (
        lax.all_gather(ssd_out, "tp", axis=1, tiled=True),
        lax.all_gather(pool_out, "tp", axis=1, tiled=True),
    )
    own_half = jnp.zeros((tok_rows, half_width), jnp.float32)
    for part_index in range(core_count):
        part_sum = jnp.dot(
            every_ssd[:, part_index * inner_local : (part_index + 1) * inner_local],
            rows_ssd[part_index * inner_local : (part_index + 1) * inner_local],
            preferred_element_type=jnp.float32,
        )
        part_sum = part_sum + jnp.dot(
            every_pool[:, part_index * pool_local : (part_index + 1) * pool_local],
            rows_pool[part_index * pool_local : (part_index + 1) * pool_local],
            preferred_element_type=jnp.float32,
        )
        own_half = own_half + part_sum.astype(jnp.bfloat16).astype(jnp.float32)
    row_squares = lax.psum(jnp.sum(own_half * own_half, axis=1), "tp")
    result = own_half * lax.rsqrt(row_squares / D + eps)[:, None] * gain_out
    return result.astype(jnp.bfloat16)[None]


def solution(mesh):
    in_specs = (
        P("fs", "sp", "tp"),
        P("fs", "sp", "tp"),
        P("fs", "sp", "tp"),
        P("fs", "sp", "tp"),
        P("fs", "sp", "tp"),
        P("fs", "sp", "tp"),
        P(),
        P(),
        P(),
        P(),
        P(),
        P(),
        P("fs", "sp", "tp"),
        P(),
        P(),
        P("tp", ("sp", "fs")),
        P("tp", ("sp", "fs")),
        P(),
    )
    out_specs = P("fs", "sp", "tp")
    return jax.shard_map(body, mesh=mesh, in_specs=in_specs, out_specs=out_specs, check_vma=False)
```

profile of v0, /device:TPU:25, one launch (start us, length us, event | category | flops | bytes accessed | tf_op | source)
XLA Modules:
  0.0 290.5 jit_solution(15163872265575039758)
XLA Ops:
  6.6 1.5 copy.117
  8.3 1.3 collective-permute-start
  9.7 1.3 collective-permute-start.2
  11.7 0.6 slice_reduce_fusion
  12.6 0.7 dynamic-slice_convert_fusion.9
  13.4 4.1 %collective-permute-done.2 = bf16[3,256]{1,0:T(4,128)(2,1)S(1)} collective-permute-done((bf16[3,256]{1,0:T(4,128)(2,1)S(1)}, bf16[3,256]{1,0:T(4,128)(2,1)S(1)}, u32[]{:S(2)}, u32[]{:S(2)}) %collective-permute-start.2) | collective-permute-done | bytes 1568 | tf_op jit(solution)/shard_map/ppermute | solution.py:21
  17.8 0.5 maximum_convert_fusion
  18.3 2.9 multiply_convert_fusion.4
  21.2 2.4 reshape.212
  23.6 0.5 multiply_convert_fusion.2
  24.1 0.4 copy-done.1
  24.9 3.0 %while.26 = (s32[]{:T(128)}, f32[2,8,64,128]{3,2,1,0:T(8,128)S(1)}, f32[3,2,8,64,128]{4,3,2,1,0:T(8,128)}, f32[3,2,8]{2,1,0:T(2,128)S(1)}, f32[3,2,8,64,128]{4,3,2,1,0:T(8,128)S(1)}, /*index=5*/s32[]{:T(128)}, s32[]{:T(128)}) while((s32[]{:T(128)}, f32[2,8,64,128]{3,2,1,0:T(8,128)S(1)}, f32[3,2,8,64,128]{4,3,2,1,0:T(8,128)}, ...), condition=%wide.region_2.3_spmd.clone, body=%wide.region_1.2_spmd.clone.sunk | while | flops 524291 | bytes 2621740 | solution.py:184
  25.0 0.8 bitcast_dynamic-update-slice_fusion.2
  25.9 0.8 bitcast_dynamic-update-slice_fusion.2
  26.9 0.8 bitcast_dynamic-update-slice_fusion.2
  27.9 0.8 convert_element_type.290
  28.8 2.1 copy.141
  30.9 0.8 copy.145
  31.9 1.3 collective-permute-start.1
  33.2 0.7 slice_bitcast_fusion.9
  33.9 1.3 collective-permute-start.3
  35.4 0.6 fusion.20
  36.0 9.0 %all-gather.2 = bf16[4,2,8]{2,1,0:T(2,128)(2,1)S(1)} all-gather(bf16[1,2,8]{2,1,0:T(2,128)(2,1)S(1)} %bitcast.162), channel_id=2, replica_groups=mesh['sp'=4,'fs'=4,'tp'=2] {'sp'}, dimensions={0}, use_global_device_ids=true | all-gather | bytes 160 | tf_op jit(solution)/shard_map/all_gather | solution.py:27
  45.3 0.4 copy.138
  45.8 1.7 reshape.233
  48.2 0.6 copy-done.2
  48.8 2.6 fusion.2
  51.5 6.0 %all-gather.14.cloned.1.call-done = bf16[8,8,64,128]{3,2,1,0:T(8,128)(2,1)} async-done(((bf16[2,8,64,128]{3,2,1,0:T(8,128)(2,1)}), bf16[8,8,64,128]{3,2,1,0:T(8,128)(2,1)}) %all-gather.14.cloned.1.call-update) | async-done | bytes 1048592 | tf_op jit(solution)/shard_map/all_gather | solution.py:27
  57.6 3.6 %while.25 = (s32[]{:T(128)}, f32[2,8,64,128]{3,2,1,0:T(8,128)S(1)}, s32[]{:T(128)}, bf16[4,2,8]{2,1,0:T(2,128)(2,1)S(1)}, bf16[4,2,8,64,128]{4,3,2,1,0:T(8,128)(2,1)}, /*index=5*/s32[]{:T(128)}, s32[]{:T(128)}, s32[]{:T(128)}) while((s32[]{:T(128)}, f32[2,8,64,128]{3,2,1,0:T(8,128)S(1)}, s32[]{:T(128)}, bf16[4,2,8]{2,1,0:T(2,128)(2,1)S(1)}, ...), condition=%wide.region_6.7_spmd, body=%wide.region_5.6_spmd.sunk | while | flops 393237 | bytes 1311015 | solution.py:41
  57.6 1.1 convert_add_fusion.4
  58.8 1.1 convert_add_fusion.4
  59.9 1.1 convert_add_fusion.4
  61.2 3.3 %multiply_reduce_fusion.1 = (f32[3,128,2]{1,2,0:T(2,128)S(1)}, f32[3,128,2,8,64]{1,4,3,2,0:T(8,128)S(1)}) fusion(f32[3,128,2,8,64]{1,0,4,3,2:T(4,128)} %reshape.233, f32[3,128,2,8]{1,3,2,0:T(8,128)S(1)} %copy.136, bf16[3,128,2,128,1]{3,2,1,0,4:T(2,128)(2,1)S(1)} %bitcast.147, f32[3,2,8,64,128]{4,3,2,1,0:T(8,128)} %get-tuple-element.77, ...), kind=kOutput, calls=%fused_computation.38 | convolution fusion | flops 105381120 | bytes 7040192 | tf_op jit(solution)/shard_map/ktgn,kgepn->ktgep/dot_general | solution.py:198
  64.5 1.1 copy.137
  65.7 1.4 fusion.6
  67.4 1.5 fusion.46
  69.3 2.5 all_gather.27
  71.8 99.9 %all-gather.10.cloned.1.call-done = bf16[1024,4096]{0,1:T(8,128)(2,1)} async-done(((bf16[1024,256]{0,1:T(8,128)(2,1)}), bf16[1024,4096]{0,1:T(8,128)(2,1)}) %all-gather.10.cloned.1.call-update) | async-done | bytes 8388624 | tf_op jit(solution)/shard_map/all_gather | solution.py:218
  171.7 7.6 %all-to-all-start = ((bf16[1024,2,2048]{0,2,1:T(8,128)(2,1)}), bf16[1024,2,2048]{0,2,1:T(8,128)(2,1)}, u32[]{:S(2)}, u32[]{:S(2)}) async-start(bf16[1024,2,2048]{0,2,1:T(8,128)(2,1)} %bitcast.137), calls=%async_computation | async-start | bytes 16777216 | tf_op jit(solution)/shard_map/all_to_all | solution.py:222
  179.4 68.6 %all-gather.12.cloned.1.call-done = bf16[512,4096]{0,1:T(8,128)(2,1)} async-done(((bf16[512,256]{0,1:T(8,128)(2,1)}), bf16[512,4096]{0,1:T(8,128)(2,1)}) %all-gather.12.cloned.1.call-update) | async-done | bytes 4194320 | tf_op jit(solution)/shard_map/all_gather | solution.py:219
  248.0 7.0 %all-to-all-start.1 = ((bf16[512,2,2048]{0,2,1:T(8,128)(2,1)}), bf16[512,2,2048]{0,2,1:T(8,128)(2,1)}, u32[]{:S(2)}, u32[]{:S(2)}) async-start(bf16[512,2,2048]{0,2,1:T(8,128)(2,1)} %bitcast.142), calls=%async_computation.1 | async-start | bytes 8388608 | tf_op jit(solution)/shard_map/all_to_all | solution.py:223
  255.0 5.7 %all-gather.8.cloned.1.call-done = bf16[384,2048]{0,1:T(8,128)(2,1)} async-done(((bf16[384,1024]{0,1:T(8,128)(2,1)}), bf16[384,2048]{0,1:T(8,128)(2,1)}) %all-gather.8.cloned.1.call-update) | async-done | bytes 1572880 | tf_op jit(solution)/shard_map/all_gather | solution.py:226
  260.7 5.9 %fusion.1 = f32[384,2048]{1,0:T(8,128)} fusion(bf16[2,1024,2048]{1,2,0:T(8,128)(2,1)} %bitcast.33, bf16[384,2048]{0,1:T(8,128)(2,1)} %all-gather.8.cloned.1.call-done), kind=kOutput, calls=%fused_computation.8 | convolution fusion | flops 1610612736 | bytes 8126464 | tf_op jit(solution)/shard_map/dot_general | solution.py:231
  266.6 3.7 %add_convert_fusion.1 = bf16[384,2048]{1,0:T(8,128)(2,1)S(1)} fusion(f32[384,2048]{1,0:T(8,128)} %fusion.1, bf16[2,512,2048]{1,2,0:T(8,128)(2,1)} %bitcast.40, bf16[384,1024]{0,1:T(8,128)(2,1)S(1)} %all_gather.27), kind=kOutput, calls=%fused_computation.13 | convolution fusion | flops 806879232 | bytes 7208960 | tf_op jit(solution)/shard_map/dot_general | solution.py:236
  270.3 4.0 %fusion = f32[384,2048]{1,0:T(8,128)S(1)} fusion(bf16[2,1024,2048]{1,2,0:T(8,128)(2,1)} %bitcast.33, bf16[384,2048]{0,1:T(8,128)(2,1)S(1)} %copy-done.23), kind=kOutput, calls=%fused_computation.6 | convolution fusion | flops 1610612736 | bytes 8126464 | tf_op jit(solution)/shard_map/dot_general | solution.py:231
  274.3 3.9 %multiply_reduce_fusion = (f32[384]{0:T(512)S(1)}, bf16[384,2048]{1,0:T(8,128)(2,1)}) fusion(bf16[384,2048]{1,0:T(8,128)(2,1)S(1)} %add_convert_fusion.1, f32[384,2048]{1,0:T(8,128)S(1)} %fusion, bf16[2,512,2048]{1,2,0:T(8,128)(2,1)} %bitcast.40, bf16[384,1024]{0,1:T(8,128)(2,1)S(1)} %all_gather.27), kind=kOutput, calls=%fused_computation.10 | convolution fusion | flops 810811008 | bytes 8783360 | tf_op jit(solution)/shard_map/dot_general | solution.py:236
  278.2 2.5 psum.7
  280.7 3.3 %fusion.3 = bf16[1,384,2048]{2,1,0:T(8,128)(2,1)} fusion(bf16[384,2048]{1,0:T(8,128)(2,1)} %get-tuple-element.137, bf16[384,2048]{1,0:T(8,128)(2,1)S(1)} %add_convert_fusion.1, f32[2048]{0:T(1024)S(1)} %dynamic-slice_convert_fusion.4, f32[384]{0:T(512)S(1)} %add_rsqrt_fusion), kind=kLoop, calls=%fused_computation.19 | loop fusion | flops 4718592 | bytes 4728320 | tf_op jit(solution)/shard_map/broadcast_in_dim | solution.py:244
  (118 shorter events, 4.5 us)
Async XLA Ops:
  6.5 62.3 %copy-start = (bf16[4,256,256]{2,1,0:T(8,128)(2,1)S(1)}, bf16[4,256,256]{2,1,0:T(8,128)(2,1)}, u32[]{:S(2)}) copy-start(bf16[4,256,256]{2,1,0:T(8,128)(2,1)} %param.35) | copy-start | bytes 1572868
  6.5 3.1 %copy-start.6 = (bf16[1,384,256]{2,1,0:T(8,128)(2,1)S(1)}, bf16[1,384,256]{2,1,0:T(8,128)(2,1)}, u32[]{:S(2)}) copy-start(bf16[1,384,256]{2,1,0:T(8,128)(2,1)} %param.24) | copy-start | bytes 589828
  6.5 4.4 %copy-start.8 = (f32[1,384,16]{1,2,0:T(8,128)S(1)}, f32[1,384,16]{1,2,0:T(8,128)}, u32[]{:S(2)}) copy-start(f32[1,384,16]{1,2,0:T(8,128)} %param.27) | copy-start | bytes 73732
  6.5 4.5 %copy-start.24 = (f32[32]{0:T(128)S(1)}, f32[32]{0:T(128)}, u32[]{:S(2)}) copy-start(f32[32]{0:T(128)} %param.28) | copy-start | bytes 388
  6.5 4.6 %copy-start.10 = (bf16[1,384,16]{1,2,0:T(8,128)(2,1)S(1)}, bf16[1,384,16]{1,2,0:T(8,128)(2,1)}, u32[]{:S(2)}) copy-start(bf16[1,384,16]{1,2,0:T(8,128)(2,1)} %param.26) | copy-start | bytes 36868
  6.5 51.0 %all-gather.14.cloned.1.call-start = ((), (), s32[]{:S(2)}) async-start(), calls=%async_computation.5 | async-start | bytes 1310720 | tf_op jit(solution)/shard_map/all_gather | solution.py:27
  8.1 4.3 %copy-start.9 = (bf16[4,2048]{1,0:T(4,128)(2,1)S(1)}, bf16[4,2048]{1,0:T(4,128)(2,1)}, u32[]{:S(2)}) copy-start(bf16[4,2048]{1,0:T(4,128)(2,1)} %param.29) | copy-start | bytes 49156
  8.2 4.4 %copy-start.15 = (bf16[4,512]{1,0:T(4,128)(2,1)S(1)}, bf16[4,512]{1,0:T(4,128)(2,1)}, u32[]{:S(2)}) copy-start(bf16[4,512]{1,0:T(4,128)(2,1)} %param.30) | copy-start | bytes 12292
  8.2 4.4 %copy-start.16 = (bf16[4,512]{1,0:T(4,128)(2,1)S(1)}, bf16[4,512]{1,0:T(4,128)(2,1)}, u32[]{:S(2)}) copy-start(bf16[4,512]{1,0:T(4,128)(2,1)} %param.31) | copy-start | bytes 12292
  8.2 5.1 %copy-start.22 = (bf16[512]{0:T(512)(128)(2,1)S(1)}, bf16[512]{0:T(512)(128)(2,1)}, u32[]{:S(2)}) copy-start(bf16[512]{0:T(512)(128)(2,1)} %param.32) | copy-start | bytes 3076
  8.3 9.5 %collective-permute-start = (bf16[3,1024]{0,1:T(8,128)(2,1)S(1)}, bf16[3,1024]{0,1:T(8,128)(2,1)S(1)}, u32[]{:S(2)}, u32[]{:S(2)}) collective-permute-start(bf16[3,1024]{0,1:T(8,128)(2,1)S(1)} %slice_bitcast_fusion.8), channel_id=1, source_target_pairs={{0,8},{8,16},{16,24},{1,9},{9,17},{17,25},{2,10},{10,18},{18,26},{... | collective-permute-start | bytes 18440 | tf_op jit(solution)/shard_map/ppermute | solution.py:21
  9.7 7.8 %collective-permute-start.2 = (bf16[3,256]{1,0:T(4,128)(2,1)S(1)}, bf16[3,256]{1,0:T(4,128)(2,1)S(1)}, u32[]{:S(2)}, u32[]{:S(2)}) collective-permute-start(bf16[3,256]{1,0:T(4,128)(2,1)S(1)} %slice_bitcast_fusion.11), channel_id=1, source_target_pairs={{0,8},{8,16},{16,24},{1,9},{9,17},{17,25},{2,10},{10,18},{18,26},{... | collective-permute-start | bytes 4616 | tf_op jit(solution)/shard_map/ppermute | solution.py:21
  23.6 1.0 copy-start.1
  27.9 3.0 %copy-start.5 = (bf16[512,256]{1,0:T(8,128)(2,1)S(1)}, bf16[512,256]{1,0:T(8,128)(2,1)}, u32[]{:S(2)}) copy-start(bf16[512,256]{1,0:T(8,128)(2,1)} %param.38) | copy-start | bytes 786436
  27.9 3.9 %copy-start.7 = (bf16[1,384,256]{2,1,0:T(8,128)(2,1)S(1)}, bf16[1,384,256]{2,1,0:T(8,128)(2,1)}, u32[]{:S(2)}) copy-start(bf16[1,384,256]{2,1,0:T(8,128)(2,1)} %param.25) | copy-start | bytes 589828
  27.9 7.4 %copy-start.20 = (bf16[2048]{0:T(1024)(128)(2,1)S(1)}, bf16[2048]{0:T(1024)(128)(2,1)}, u32[]{:S(2)}) copy-start(bf16[2048]{0:T(1024)(128)(2,1)} %param.33) | copy-start | bytes 12292
  27.9 7.4 %copy-start.18 = (bf16[4096]{0:T(1024)(128)(2,1)S(1)}, bf16[4096]{0:T(1024)(128)(2,1)}, u32[]{:S(2)}) copy-start(bf16[4096]{0:T(1024)(128)(2,1)} %param.39) | copy-start | bytes 24580
  28.7 7.3 %copy-start.19 = (bf16[2,8]{1,0:T(2,128)(2,1)S(1)}, bf16[2,8]{1,0:T(2,128)(2,1)}, u32[]{:S(2)}) copy-start(bf16[2,8]{1,0:T(2,128)(2,1)} %get-tuple-element.118) | copy-start | bytes 100
  28.7 143.0 %all-gather.10.cloned.1.call-start = ((), (), s32[]{:S(2)}) async-start(), calls=%async_computation.3 | async-start | bytes 8912896 | tf_op jit(solution)/shard_map/all_gather | solution.py:218
  30.8 14.5 %copy-start.4 = (bf16[1,384,1024]{2,1,0:T(8,128)(2,1)S(1)}, bf16[1,384,1024]{2,1,0:T(8,128)(2,1)}, u32[]{:S(2)}) copy-start(bf16[1,384,1024]{2,1,0:T(8,128)(2,1)} %param.23) | copy-start | bytes 2359300
  30.9 217.1 %all-gather.12.cloned.1.call-start = ((), (), s32[]{:S(2)}) async-start(), calls=%async_computation.4 | async-start | bytes 4456448 | tf_op jit(solution)/shard_map/all_gather | solution.py:219
  31.8 228.9 %all-gather.8.cloned.1.call-start = ((), (), s32[]{:S(2)}) async-start(), calls=%async_computation.2 | async-start | bytes 2359296 | tf_op jit(solution)/shard_map/all_gather | solution.py:226
  31.9 15.7 %collective-permute-start.1 = (bf16[3,256]{1,0:T(4,128)(2,1)S(1)}, bf16[3,256]{1,0:T(4,128)(2,1)S(1)}, u32[]{:S(2)}, u32[]{:S(2)}) collective-permute-start(bf16[3,256]{1,0:T(4,128)(2,1)S(1)} %slice_bitcast_fusion.12), channel_id=1, source_target_pairs={{0,8},{8,16},{16,24},{1,9},{9,17},{17,25},{2,10},{10,18},{18,26},{... | collective-permute-start | bytes 4616 | tf_op jit(solution)/shard_map/ppermute | solution.py:21
  33.9 33.3 %collective-permute-start.3 = (bf16[15,512]{1,0:T(8,128)(2,1)S(1)}, bf16[15,512]{1,0:T(8,128)(2,1)S(1)}, u32[]{:S(2)}, u32[]{:S(2)}) collective-permute-start(bf16[15,512]{1,0:T(8,128)(2,1)S(1)} %slice_bitcast_fusion.9), channel_id=1, source_target_pairs={{0,8},{8,16},{16,24},{1,9},{9,17},{17,25},{2,10},{10,18},{18,26},{... | collective-permute-start | bytes 46088 | tf_op jit(solution)/shard_map/ppermute | solution.py:21
  45.7 1.9 copy-start.11
  45.7 1.9 copy-start.12
  45.7 1.9 copy-start.13
  45.7 1.9 copy-start.14
  47.6 1.2 copy-start.2
  57.6 3.7 %copy-start.17 = (f32[3,2,8]{2,1,0:T(2,128)S(1)}, f32[3,2,8]{2,1,0:T(2,128)}, u32[]{:S(2)}) copy-start(f32[3,2,8]{2,1,0:T(2,128)} %fusion.20) | copy-start | bytes 580
  65.7 1.5 copy-start.21
  65.7 1.6 copy-start.3
  171.7 76.2 %all-to-all-start = ((bf16[1024,2,2048]{0,2,1:T(8,128)(2,1)}), bf16[1024,2,2048]{0,2,1:T(8,128)(2,1)}, u32[]{:S(2)}, u32[]{:S(2)}) async-start(bf16[1024,2,2048]{0,2,1:T(8,128)(2,1)} %bitcast.137), calls=%async_computation | async-start | bytes 16777216 | tf_op jit(solution)/shard_map/all_to_all | solution.py:222
  248.0 18.6 %all-to-all-start.1 = ((bf16[512,2,2048]{0,2,1:T(8,128)(2,1)}), bf16[512,2,2048]{0,2,1:T(8,128)(2,1)}, u32[]{:S(2)}, u32[]{:S(2)}) async-start(bf16[512,2,2048]{0,2,1:T(8,128)(2,1)} %bitcast.142), calls=%async_computation.1 | async-start | bytes 8388608 | tf_op jit(solution)/shard_map/all_to_all | solution.py:223
  266.6 3.7 %copy-start.23 = (bf16[384,2048]{0,1:T(8,128)(2,1)S(1)}, bf16[384,2048]{0,1:T(8,128)(2,1)}, u32[]{:S(2)}) copy-start(bf16[384,2048]{0,1:T(8,128)(2,1)} %all-gather.8.cloned.1.call-done) | copy-start | bytes 4718596
Sparse Core Ops, SparseCore 0:
  28.9 28.6 all-gather.13
  60.3 111.4 all-gather.9
  174.5 73.4 all-gather.11
  249.4 11.2 all-gather.7
where the time goes:
time: 293 us; the launch traced here: 291 us
  waiting for transfers between devices  184 us (63%)
  matrix products  24.4 us (8%)
  other arithmetic  20.5 us (7%)
  starting transfers between devices  20 us (7%)
  blocking collectives  14 us (5%)
  between operations  13.8 us (5%)
  local copies, waits for them, and re-layouts  13.1 us (4%)
    all_gather x1, waiting for transfers between devices, body(): lax.all_gather(statespace_output_weight, ('sp', 'fs'), axis=1, tiled=True)  99.9 us
    all_gather x1, waiting for transfers between devices, body(): lax.all_gather(pooling_output_weight, ('sp', 'fs'), axis=1, tiled=True)  68.6 us
    dot_general x2, matrix products, body(): jnp.dot(every_ssd[:, part_index * inner_local:(part_index + 1) * inner_lo...  9.94 us
    all_gather x1, blocking collectives, entering_2(): lax.all_gather(a.astype(kind), axis)  8.99 us
    all_to_all x1, starting transfers between devices, body(): lax.all_to_all(whole_ssd, 'tp', split_axis=1, concat_axis=0, tiled=True)  7.64 us
    dot_general x2, matrix products, body(): jnp.dot(every_pool[:, part_index * pool_local:(part_index + 1) * pool_loc...  7.58 us
    all_to_all x1, starting transfers between devices, body(): lax.all_to_all(whole_pool, 'tp', split_axis=1, concat_axis=0, tiled=True)  7.04 us
    all_gather x1, waiting for transfers between devices, entering_2(): lax.all_gather(a.astype(kind), axis)  6.03 us
  transfers between devices with their start and end apart: 10, of which 5 were waited for; matrix products, arithmetic and copies ran while one was open for 10% of the time, Pallas kernels for 0%

commit v1 on v0

--- a/solution.py
+++ b/solution.py
@@ -1,6 +1,10 @@
+import functools
+
 import jax
 import jax.numpy as jnp
 from jax import lax
+from jax.experimental import pallas as pl
+from jax.experimental.pallas import tpu as pltpu
 from jax.sharding import PartitionSpec as P
 
 D = 4096
@@ -39,6 +43,179 @@
         )
 
     return lax.fori_loop(0, place, one, state)
+
+
+MESH_IDS = pl.DeviceIdType.MESH
+
+
+def ring_place(index, size):
+    if size != 4:
+        return index
+    return index + (index // 2) * (1 - 2 * (index % 2))
+
+
+class Ring:
+    def __init__(self, axis, size, folded):
+        self.axis, self.size, self.folded = axis, size, folded
+        me = lax.axis_index(axis)
+        self.place = ring_place(me, size) if folded else me
+
+    def at(self, offset):
+        spot = lax.rem(self.place + offset + 2 * self.size, self.size)
+        return ring_place(spot, self.size) if self.folded else spot
+
+    def hops(self):
+        found = []
+        for step in range(1, self.size // 2 + 1):
+            halved = self.size % 2 == 0 and step == self.size // 2
+            found.append((step, 1, halved))
+            found.append((step, -1, halved))
+        return found
+
+    def offsets(self):
+        found = [0]
+        for step, way, halved in self.hops():
+            if not (halved and way == -1):
+                found.append(-way * step)
+        return found
+
+
+class Gather:
+    def __init__(self, own, whole, sends, arrivals, sp_size, fs_size):
+        self.own, self.whole = own, whole
+        self.sends, self.arrivals = sends, arrivals
+        self.count = 0
+        self.width = own.shape[1]
+        self.fs_size = fs_size
+        self.sp = Ring("sp", sp_size, False)
+        self.fs = Ring("fs", fs_size, True)
+        self.live = {}
+
+    def columns(self, sp_off, fs_off):
+        at = (self.sp.at(sp_off) * self.fs_size + self.fs.at(fs_off)) * self.width
+        return pl.ds(pl.multiple_of(at, self.width), self.width)
+
+    def start(self, key, ring, way, rows, sp_off, fs_off):
+        first = sp_off == 0 and fs_off == 0
+        cols = self.columns(sp_off, fs_off)
+        src = self.own.at[rows] if first else self.whole.at[rows, cols]
+        copy = pltpu.make_async_remote_copy(
+            src_ref=src,
+            dst_ref=self.whole.at[rows, cols],
+            send_sem=self.sends.at[self.count],
+            recv_sem=self.arrivals.at[self.count],
+            device_id={ring.axis: ring.at(way)},
+            device_id_type=MESH_IDS,
+        )
+        copy.start()
+        self.count += 1
+        self.live[key] = copy
+
+    def barrier(self):
+        barrier = pltpu.get_barrier_semaphore()
+        total = 0
+        for ring in (self.sp, self.fs):
+            if ring.size > 1:
+                for way in (1, -1):
+                    pl.semaphore_signal(
+                        barrier, inc=1, device_id={ring.axis: ring.at(way)}, device_id_type=MESH_IDS
+                    )
+                    total += 1
+        if total:
+            pl.semaphore_wait(barrier, total)
+
+    def send(self, part, stage, cross, step, way, halved):
+        rows_all = self.own.shape[0]
+        low, high = (0, rows_all // 2) if part == 0 else (rows_all // 2, rows_all)
+        ring = (self.fs, self.sp)[(part + stage) % 2]
+        if halved:
+            mid = low + (high - low) // 2
+            low, high = (low, mid) if way == 1 else (mid, high)
+        off = -way * (step - 1)
+        sp_off, fs_off = (off, cross) if ring is self.sp else (cross, off)
+        self.start((part, stage, cross, step, way), ring, way, pl.ds(low, high - low), sp_off, fs_off)
+
+    def run(self):
+        first = [(self.fs, self.sp)[part] for part in (0, 1)]
+        then = [(self.sp, self.fs)[part] for part in (0, 1)]
+
+        def send_at(stage, part, cross, step):
+            ring = (first, then)[stage][part]
+            for s, way, halved in ring.hops():
+                if s == step:
+                    self.send(part, stage, cross, s, way, halved)
+
+        def wait_at(stage, part, cross, step):
+            ring = (first, then)[stage][part]
+            for s, way, halved in ring.hops():
+                if s == step:
+                    self.live[(part, stage, cross, s, way)].wait_recv()
+
+        last = max(self.sp.size, self.fs.size) // 2
+        for part in (0, 1):
+            send_at(0, part, 0, 1)
+        for part in (0, 1):
+            send_at(1, part, 0, 1)
+        for step in range(1, last + 1):
+            for part in (0, 1):
+                wait_at(0, part, 0, step)
+                send_at(0, part, 0, step + 1)
+            for part in (0, 1):
+                for off in first[part].offsets():
+                    if off and abs(off) == step:
+                        send_at(1, part, off, 1)
+        for step in range(1, last + 1):
+            deepest = max(len(ring.offsets()) for ring in first)
+            for spot in range(deepest):
+                for part in (0, 1):
+                    offsets = first[part].offsets()
+                    if spot < len(offsets):
+                        wait_at(1, part, offsets[spot], step)
+                        send_at(1, part, offsets[spot], step + 1)
+
+    def finish(self):
+        for copy in self.live.values():
+            copy.wait_send()
+
+
+def hop_count(sp_size, fs_size):
+    def hops(size):
+        return 2 * (size // 2)
+
+    return hops(sp_size) * (1 + fs_size) + hops(fs_size) * (1 + sp_size)
+
+
+def gather_kernel(sp_size, fs_size, own, whole, sends, arrivals, local_sem):
+    gather = Gather(own, whole, sends, arrivals, sp_size, fs_size)
+    gather.barrier()
+    mine = pltpu.make_async_copy(own, whole.at[:, gather.columns(0, 0)], local_sem)
+    mine.start()
+    gather.run()
+    mine.wait()
+    gather.finish()
+
+
+def gathered_columns(own):
+    sp_size, fs_size = lax.axis_size("sp"), lax.axis_size("fs")
+    rows, width = own.shape
+    if width % 128 or rows % 64:
+        return lax.all_gather(own, ("sp", "fs"), axis=1, tiled=True)
+    hops = hop_count(sp_size, fs_size)
+    return pl.pallas_call(
+        functools.partial(gather_kernel, sp_size, fs_size),
+        out_shape=jax.ShapeDtypeStruct((rows, width * sp_size * fs_size), own.dtype),
+        in_specs=[pl.BlockSpec(memory_space=pltpu.VMEM)],
+        out_specs=pl.BlockSpec(memory_space=pltpu.VMEM),
+        scratch_shapes=[
+            pltpu.SemaphoreType.DMA((hops,)),
+            pltpu.SemaphoreType.DMA((hops,)),
+            pltpu.SemaphoreType.DMA,
+        ],
+        compiler_params=pltpu.CompilerParams(
+            collective_id=0, has_side_effects=True, vmem_limit_bytes=40 * 2**20
+        ),
+        name="gather_columns",
+    )(own)
 
 
 def causal_taps(input_rows, prior_rows, tap_weights, offset_bias):
@@ -118,15 +295,25 @@
     groups_pool = pool_local // POOL_GROUP
     pool_tail = 2**POOL_GROUPS - 1
     conv_tail = CONV - 1
-    prior_x, prior_b, prior_c, prior_pool = passed_along(
-        (
-            head_channel_rows[tok_rows - conv_tail :],
-            input_projection_rows[tok_rows - conv_tail :],
-            output_projection_rows[tok_rows - conv_tail :],
-            pooling_rows[tok_rows - pool_tail :],
-        ),
-        "sp",
-        1,
+    own_columns = jnp.concatenate([statespace_output_weight, pooling_output_weight], axis=0)
+    whole_columns = gathered_columns(own_columns)
+    tails = jnp.concatenate(
+        [
+            jnp.pad(rows[tok_rows - tail :], ((pool_tail - tail, 0), (0, 0)))
+            for rows, tail in (
+                (head_channel_rows, conv_tail),
+                (input_projection_rows, conv_tail),
+                (output_projection_rows, conv_tail),
+                (pooling_rows, pool_tail),
+            )
+        ],
+        axis=1,
+    )
+    prior = passed_along(tails, "sp", 1)
+    widths = (inner_local, state_local, state_local, pool_local)
+    prior_x, prior_b, prior_c, prior_pool = (
+        prior[pool_tail - tail :, sum(widths[:at]) : sum(widths[: at + 1])]
+        for at, tail in enumerate((conv_tail, conv_tail, conv_tail, pool_tail))
     )
     taps_x = lax.dynamic_slice_in_dim(head_channel_taps, core_index * inner_local, inner_local, 1)
     taps_b = lax.dynamic_slice_in_dim(
@@ -214,31 +401,18 @@
     gain_out = lax.dynamic_slice_in_dim(
         output_norm_gain, core_index * half_width, half_width, 0
     ).astype(jnp.float32)
-    whole_ssd, whole_pool = (
-        lax.all_gather(statespace_output_weight, ("sp", "fs"), axis=1, tiled=True),
-        lax.all_gather(pooling_output_weight, ("sp", "fs"), axis=1, tiled=True),
-    )
-    rows_ssd, rows_pool = (
-        lax.all_to_all(whole_ssd, "tp", split_axis=1, concat_axis=0, tiled=True),
-        lax.all_to_all(whole_pool, "tp", split_axis=1, concat_axis=0, tiled=True),
-    )
-    every_ssd, every_pool = (
-        lax.all_gather(ssd_out, "tp", axis=1, tiled=True),
-        lax.all_gather(pool_out, "tp", axis=1, tiled=True),
-    )
-    own_half = jnp.zeros((tok_rows, half_width), jnp.float32)
-    for part_index in range(core_count):
-        part_sum = jnp.dot(
-            every_ssd[:, part_index * inner_local : (part_index + 1) * inner_local],
-            rows_ssd[part_index * inner_local : (part_index + 1) * inner_local],
-            preferred_element_type=jnp.float32,
-        )
-        part_sum = part_sum + jnp.dot(
-            every_pool[:, part_index * pool_local : (part_index + 1) * pool_local],
-            rows_pool[part_index * pool_local : (part_index + 1) * pool_local],
-            preferred_element_type=jnp.float32,
-        )
-        own_half = own_half + part_sum.astype(jnp.bfloat16).astype(jnp.float32)
+    channels = jnp.concatenate([ssd_out, pool_out], axis=1)
+    partial = jnp.dot(channels, whole_columns, preferred_element_type=jnp.float32).astype(
+        jnp.bfloat16
+    )
+    own_half = lax.dynamic_slice_in_dim(partial, core_index * half_width, half_width, 1).astype(
+        jnp.float32
+    )
+    for hop in range(1, core_count):
+        target = lax.rem(core_index + hop, core_count)
+        leaving = lax.dynamic_slice_in_dim(partial, target * half_width, half_width, 1)
+        route = [(i, (i + hop) % core_count) for i in range(core_count)]
+        own_half = own_half + lax.ppermute(leaving, "tp", route).astype(jnp.float32)
     row_squares = lax.psum(jnp.sum(own_half * own_half, axis=1), "tp")
     result = own_half * lax.rsqrt(row_squares / D + eps)[:, None] * gain_out
     return result.astype(jnp.bfloat16)[None]

time: 293 us -> 253 us (0.86)
  waiting for transfers between devices: 184 us -> 25.5 us
  Pallas kernels: 0 us -> 129 us
  starting transfers between devices: 20 us -> 2.12 us
  local copies, waits for them, and re-layouts: 13.1 us -> 24.1 us
  other arithmetic: 20.5 us -> 31 us
  matrix products: 24.4 us -> 17.1 us
  blocking collectives: 14 us -> 9.29 us
    all_gather x3 -> x0, waiting for transfers between devices: 174 us -> none  [the longest x1 99.9 us: body(): lax.all_gather(statespace_output_weight, ('sp', 'fs'), axis=1, tiled=True)]
    pallas_call x0 -> x1, Pallas kernels: none -> 129 us  [gathered_columns(): pl.pallas_call(functools.partial(gather_kernel, sp_size, fs_size), out_sh...]
    all_gather x1, waiting for transfers between devices: 6.03 us -> 22.2 us  [entering_2(): lax.all_gather(a.astype(kind), axis)]
    all_to_all x2 -> x0, starting transfers between devices: 14.7 us -> none  [the longest x1 7.64 us: body(): lax.all_to_all(whole_ssd, 'tp', split_axis=1, concat_axis=0, tiled=True)]
    dot_general x4 -> x1, matrix products: 17.5 us -> 10.1 us  [body(): jnp.dot(channels, whole_columns, preferred_element_type=jnp.float32)]
    convert_element_type x8, other arithmetic: 0.06 us -> 4.8 us  [pool_mix(): running = running + padded[start_row:start_row + tok_rows] * (offset_back...]
    slice x4 -> x9, local copies, waits for them, and re-layouts: 0.87 us -> 5.6 us  [the longest x6 3.39 us: body(): prior[pool_tail - tail:, sum(widths[:at]):sum(widths[:at + 1])]]
    ppermute x4 -> x1, waiting for transfers between devices: 4.1 us -> 0.01 us  [passed_along(): return lax.ppermute(block, axis, route)]
  transfers between devices with their start and end apart: 10 -> 3, of which waited for: 5 -> 2; matrix products, arithmetic and copies ran while one was open for 10% -> 9% of each run, Pallas kernels for 0% -> 51%
where the time goes in v1:
time: 253 us; the launch traced here: 252 us
  Pallas kernels  129 us (51%)
  other arithmetic  31 us (12%)
  waiting for transfers between devices  25.5 us (10%)
  local copies, waits for them, and re-layouts  24.1 us (10%)
  matrix products  17.1 us (7%)
  between operations  14.3 us (6%)
  blocking collectives  9.29 us (4%)
    pallas_call x1, Pallas kernels, gathered_columns(): pl.pallas_call(functools.partial(gather_kernel, sp_size, fs_size), out_sh...  129 us
    all_gather x1, waiting for transfers between devices, entering_2(): lax.all_gather(a.astype(kind), axis)  22.2 us
    dot_general x1, matrix products, body(): jnp.dot(channels, whole_columns, preferred_element_type=jnp.float32)  10.1 us
    unnamed x98, local copies, waits for them, and re-layouts  8.38 us
    all_gather x1, blocking collectives, entering_2(): lax.all_gather(a.astype(kind), axis)  6.79 us
  transfers between devices with their start and end apart: 3, of which 2 were waited for; matrix products, arithmetic and copies ran while one was open for 9% of the time, Pallas kernels for 51%

profile of v1, /device:TPU:25, one launch (start us, length us, event | category | flops | bytes accessed | tf_op | source)
XLA Modules:
  0.0 252.4 jit_solution(9714017457928626128)
XLA Ops:
  6.6 0.8 slice_bitcast_fusion
  7.4 0.7 slice_bitcast_fusion.1
  8.1 0.7 slice_bitcast_fusion.3
  8.8 1.1 copy.121
  9.9 1.3 collective-permute-start
  11.2 1.5 copy.122
  16.3 0.6 compare_convert_fusion.6
  19.9 0.6 exponential_multiply_fusion
  20.5 6.8 %all-gather.2 = bf16[4,2,8]{2,1,0:T(2,128)(2,1)} all-gather(bf16[1,2,8]{2,1,0:T(2,128)(2,1)S(1)} %bitcast.139), channel_id=2, replica_groups=mesh['sp'=4,'fs'=4,'tp'=2] {'sp'}, dimensions={0}, use_global_device_ids=true | all-gather | bytes 160 | tf_op jit(solution)/shard_map/all_gather | solution.py:31
  27.3 0.7 copy.142
  28.4 1.6 reshape.223
  30.8 128.8 %gather_columns.1 = bf16[1536,4096]{1,0:T(8,128)(2,1)S(1)} custom-call(bf16[1536,256]{1,0:T(8,128)(2,1)S(1)} %pad_maximum_fusion.own), custom_call_target="tpu_custom_call" | custom-call | tf_op jit(solution)/shard_map/gather_columns/pallas_call | solution.py:204
  159.6 4.5 %copy-done.1 = bf16[1536,4096]{1,0:T(8,128)(2,1)} copy-done((bf16[1536,4096]{1,0:T(8,128)(2,1)}, bf16[1536,4096]{1,0:T(8,128)(2,1)S(1)}, u32[]{:S(2)}) %copy-start.1) | copy-done | bytes 12582936
  164.2 0.7 dynamic-slice_convert_fusion.12
  165.0 0.7 fusion.76
  165.8 1.1 slice.212
  167.3 2.9 %multiply_convert_fusion.4 = bf16[384,1024]{0,1:T(8,128)(2,1)} fusion(f32[387,1024]{0,1:T(8,128)S(1)} %maximum_convert_fusion, f32[1024]{0:T(1024)S(1)} %bitcast.130, f32[1024]{0:T(1024)S(1)} %bitcast.128, f32[1024]{0:T(1024)S(1)} %bitcast.129, f32[1024]{0:T(1024)S(1)} %bitcast.127), kind=kLoop, calls=%fused_computation.38 | loop fusion | flops 4718592 | bytes 7094272 | tf_op jit(solution)/shard_map/convert_element_type | solution.py:230
  170.2 2.4 reshape.202
  172.7 1.1 fusion.82
  174.2 0.7 reshape.204
  176.2 3.0 %while.26 = (s32[]{:T(128)}, f32[2,8,64,128]{3,2,1,0:T(8,128)S(1)}, f32[3,2,8,64,128]{4,3,2,1,0:T(8,128)}, f32[3,2,8]{2,1,0:T(2,128)S(1)}, f32[3,2,8,64,128]{4,3,2,1,0:T(8,128)S(1)}, /*index=5*/s32[]{:T(128)}, s32[]{:T(128)}) while((s32[]{:T(128)}, f32[2,8,64,128]{3,2,1,0:T(8,128)S(1)}, f32[3,2,8,64,128]{4,3,2,1,0:T(8,128)}, ...), condition=%wide.region_2.3_spmd.clone, body=%wide.region_1.2_spmd.clone.sunk | while | flops 524291 | bytes 2622240 | solution.py:371
  176.2 0.8 bitcast_dynamic-update-slice_fusion.2
  177.2 0.8 bitcast_dynamic-update-slice_fusion.2
  178.2 0.8 bitcast_dynamic-update-slice_fusion.2
  179.2 0.8 convert_element_type.292
  180.1 1.0 maximum_convert_fusion.2
  181.9 0.9 slice.228
  183.3 1.5 fusion.45
  185.3 0.7 copy-done.4
  185.9 2.7 %fusion = f32[3,2,8,64,128]{4,3,2,1,0:T(8,128)} fusion(f32[3,2,8,128]{3,2,1,0:T(8,128)S(1)} %copy-done.14, f32[3,2,8,128]{3,2,1,0:T(8,128)S(1)} %copy.134, f32[3,2,128,128]{3,2,1,0:T(8,128)S(1)} %fusion.59, pred[128,128]{1,0:T(8,128)(4,1)S(1)} %iota_compare_fusion.5, bf16[3,128,2,8,64]{1,0,4,3,2:T(4,128)(2,1)S(1)} %copy-done.4), kind=kOutput, calls=%fused_computation.11 | convolution fusion | flops 105381888 | bytes 2818048 | tf_op jit(solution)/shard_map/kgetu,kugep->ktgep/dot_general | solution.py:359
  188.6 22.2 %all-gather.5.cloned.1.call-done = bf16[8,8,64,128]{3,2,1,0:T(8,128)(2,1)} async-done(((bf16[2,8,64,128]{3,2,1,0:T(8,128)(2,1)}), bf16[8,8,64,128]{3,2,1,0:T(8,128)(2,1)}) %all-gather.5.cloned.1.call-update) | async-done | bytes 1048592 | tf_op jit(solution)/shard_map/all_gather | solution.py:31
  210.9 5.5 %while.25 = (s32[]{:T(128)}, f32[2,8,64,128]{3,2,1,0:T(8,128)S(1)}, s32[]{:T(128)}, bf16[4,2,8]{2,1,0:T(2,128)(2,1)}, bf16[4,2,8,64,128]{4,3,2,1,0:T(8,128)(2,1)}, /*index=5*/s32[]{:T(128)}, s32[]{:T(128)}, s32[]{:T(128)}) while((s32[]{:T(128)}, f32[2,8,64,128]{3,2,1,0:T(8,128)S(1)}, s32[]{:T(128)}, bf16[4,2,8]{2,1,0:T(2,128)(2,1)}, ...), condition=%wide.region_6.7_spmd, body=%wide.region_5.6_spmd.sunk | while | flops 393237 | bytes 1311007 | solution.py:45
  210.9 0.7 exponential_bitcast_fusion.4
  211.6 1.1 convert_add_fusion.4
  212.7 0.6 exponential_bitcast_fusion.4
  213.4 1.1 convert_add_fusion.4
  214.5 0.6 exponential_bitcast_fusion.4
  215.2 1.1 convert_add_fusion.4
  216.5 3.3 %multiply_reduce_fusion.1 = (f32[3,128,2]{1,2,0:T(2,128)S(1)}, f32[3,128,2,8,64]{1,4,3,2,0:T(8,128)S(1)}) fusion(f32[3,128,2,8,64]{1,0,4,3,2:T(4,128)} %reshape.223, f32[3,128,2,8]{1,3,2,0:T(8,128)S(1)} %copy-done.13, bf16[3,128,2,128,1]{3,2,1,0,4:T(2,128)(2,1)S(1)} %bitcast.124, f32[3,2,8,64,128]{4,3,2,1,0:T(8,128)} %get-tuple-element.77, ...), kind=kOutput, calls=%fused_computation.31 | convolution fusion | flops 105381120 | bytes 7040192 | tf_op jit(solution)/shard_map/ktgn,kgepn->ktgep/dot_general | solution.py:385
  219.8 1.1 copy.143
  221.5 10.1 %convolution_convert_fusion = bf16[384,4096]{1,0:T(8,128)(2,1)S(1)} fusion(bf16[1536,4096]{1,0:T(8,128)(2,1)} %copy-done.1, bf16[384,512]{0,1:T(8,128)(2,1)S(1)} %fusion.39, bf16[384,1024]{0,1:T(8,128)(2,1)S(1)} %fusion.4), kind=kOutput, calls=%fused_computation.5 | convolution fusion | flops 4835770368 | bytes 16908288 | tf_op jit(solution)/shard_map/dot_general | solution.py:405
  231.6 1.4 constant_dynamic-slice_fusion
  233.0 0.7 copy-done.2
  233.7 0.8 collective-permute-start.1
  234.5 3.2 %collective-permute-done.1 = bf16[384,2048]{1,0:T(8,128)(2,1)S(1)} collective-permute-done((bf16[384,2048]{1,0:T(8,128)(2,1)}, bf16[384,2048]{1,0:T(8,128)(2,1)S(1)}, u32[]{:S(2)}, u32[]{:S(2)}) %collective-permute-start.1) | collective-permute-done | bytes 1572896 | tf_op jit(solution)/shard_map/ppermute | solution.py:415
  237.8 2.0 multiply_reduce_fusion
  239.8 2.5 psum.7
  242.3 3.3 %fusion.1 = bf16[1,384,2048]{2,1,0:T(8,128)(2,1)} fusion(bf16[384,2048]{1,0:T(8,128)(2,1)S(1)} %collective-permute-done.1, f32[2048]{0:T(1024)S(1)} %dynamic-slice_convert_fusion.4, f32[384]{0:T(512)S(1)} %add_rsqrt_fusion, bf16[384,4096]{1,0:T(8,128)(2,1)} %copy-done.2, s32[]{:T(128)S(6)} %select_n.111), kind=kLoop, calls=%fused_computation.12 | loop fusion | flops 4718592 | bytes 4728324 | tf_op jit(solution)/shard_map/broadcast_in_dim | solution.py:418
  (152 shorter events, 12.4 us)
Async XLA Ops:
  6.5 178.2 %copy-start = (bf16[4,256,256]{2,1,0:T(8,128)(2,1)S(1)}, bf16[4,256,256]{2,1,0:T(8,128)(2,1)}, u32[]{:S(2)}) copy-start(bf16[4,256,256]{2,1,0:T(8,128)(2,1)} %param.35) | copy-start | bytes 1572868
  6.5 6.1 %copy-start.47 = (f32[32]{0:T(128)S(1)}, f32[32]{0:T(128)}, u32[]{:S(2)}) copy-start(f32[32]{0:T(128)} %param.28) | copy-start | bytes 388
  6.5 6.3 %copy-start.16 = (bf16[1,384,16]{1,2,0:T(8,128)(2,1)S(1)}, bf16[1,384,16]{1,2,0:T(8,128)(2,1)}, u32[]{:S(2)}) copy-start(bf16[1,384,16]{1,2,0:T(8,128)(2,1)} %param.26) | copy-start | bytes 36868
  6.5 6.3 %copy-start.12 = (f32[1,384,16]{1,2,0:T(8,128)S(1)}, f32[1,384,16]{1,2,0:T(8,128)}, u32[]{:S(2)}) copy-start(f32[1,384,16]{1,2,0:T(8,128)} %param.27) | copy-start | bytes 73732
  6.5 204.3 %all-gather.5.cloned.1.call-start = ((), (), s32[]{:S(2)}) async-start(), calls=%async_computation | async-start | bytes 1310720 | tf_op jit(solution)/shard_map/all_gather | solution.py:31
  9.9 155.9 %collective-permute-start = (bf16[15,2048]{0,1:T(8,128)(2,1)}, bf16[15,2048]{0,1:T(8,128)(2,1)}, u32[]{:S(2)}, u32[]{:S(2)}) collective-permute-start(bf16[15,2048]{0,1:T(8,128)(2,1)} %copy.121), channel_id=1, source_target_pairs={{0,8},{8,16},{16,24},{1,9},{9,17},{17,25},{2,10},{10,18},{18,26},{... | collective-permute-start | bytes 184328 | tf_op jit(solution)/shard_map/ppermute | solution.py:25
  13.2 14.9 %copy-start.8 = (bf16[1,384,1024]{2,1,0:T(8,128)(2,1)S(1)}, bf16[1,384,1024]{2,1,0:T(8,128)(2,1)}, u32[]{:S(2)}) copy-start(bf16[1,384,1024]{2,1,0:T(8,128)(2,1)} %param.23) | copy-start | bytes 2359300
  28.4 2.2 copy-start.9
  28.4 2.2 copy-start.10
  30.7 133.5 %copy-start.44 = (bf16[2048]{0:T(1024)(128)(2,1)S(1)}, bf16[2048]{0:T(1024)(128)(2,1)}, u32[]{:S(2)}) copy-start(bf16[2048]{0:T(1024)(128)(2,1)} %param.33) | copy-start | bytes 12292
  30.7 133.5 %copy-start.45 = (bf16[1024]{0:T(1024)(128)(2,1)S(1)}, bf16[1024]{0:T(1024)(128)(2,1)}, u32[]{:S(2)}) copy-start(bf16[1024]{0:T(1024)(128)(2,1)} %param.36) | copy-start | bytes 6148
  30.7 134.1 %copy-start.15 = (bf16[4,2048]{1,0:T(4,128)(2,1)S(1)}, bf16[4,2048]{1,0:T(4,128)(2,1)}, u32[]{:S(2)}) copy-start(bf16[4,2048]{1,0:T(4,128)(2,1)} %param.29) | copy-start | bytes 49156
  30.7 134.2 %copy-start.40 = (bf16[4,512]{1,0:T(4,128)(2,1)S(1)}, bf16[4,512]{1,0:T(4,128)(2,1)}, u32[]{:S(2)}) copy-start(bf16[4,512]{1,0:T(4,128)(2,1)} %param.30) | copy-start | bytes 12292
  30.8 134.2 %copy-start.41 = (bf16[4,512]{1,0:T(4,128)(2,1)S(1)}, bf16[4,512]{1,0:T(4,128)(2,1)}, u32[]{:S(2)}) copy-start(bf16[4,512]{1,0:T(4,128)(2,1)} %param.31) | copy-start | bytes 12292
  30.8 134.9 %copy-start.46 = (bf16[512]{0:T(512)(128)(2,1)S(1)}, bf16[512]{0:T(512)(128)(2,1)}, u32[]{:S(2)}) copy-start(bf16[512]{0:T(512)(128)(2,1)} %param.32) | copy-start | bytes 3076
  159.6 4.6 %copy-start.1 = (bf16[1536,4096]{1,0:T(8,128)(2,1)}, bf16[1536,4096]{1,0:T(8,128)(2,1)S(1)}, u32[]{:S(2)}) copy-start(bf16[1536,4096]{1,0:T(8,128)(2,1)S(1)} %gather_columns.1) | copy-start | bytes 37748740
  170.2 3.7 %copy-start.11 = (bf16[1,384,256]{2,1,0:T(8,128)(2,1)S(1)}, bf16[1,384,256]{2,1,0:T(8,128)(2,1)}, u32[]{:S(2)}) copy-start(bf16[1,384,256]{2,1,0:T(8,128)(2,1)} %param.24) | copy-start | bytes 589828
  172.7 2.8 %copy-start.3 = (bf16[3,128,2,8,64]{1,0,4,3,2:T(4,128)(2,1)}, bf16[3,128,2,8,64]{1,0,4,3,2:T(4,128)(2,1)S(1)}, u32[]{:S(2)}) copy-start(bf16[3,128,2,8,64]{1,0,4,3,2:T(4,128)(2,1)S(1)} %reshape.202) | copy-start | bytes 2359300
  179.2 1.9 copy-start.36
  179.2 1.9 copy-start.37
  179.2 1.9 copy-start.38
  179.2 1.9 copy-start.39
  180.0 1.7 copy-start.6
  181.1 1.8 copy-start.7
  181.4 1.7 copy-start.17
  181.4 1.7 copy-start.18
  181.4 1.7 copy-start.20
  181.4 1.7 copy-start.21
  181.5 1.7 copy-start.22
  181.5 1.7 copy-start.23
  181.5 1.7 copy-start.24
  181.5 1.7 copy-start.25
  181.5 1.7 copy-start.26
  181.5 1.7 copy-start.27
  181.5 1.7 copy-start.28
  181.5 1.7 copy-start.29
  181.5 1.7 copy-start.30
  181.5 1.7 copy-start.31
  181.6 1.7 copy-start.32
  181.6 1.7 copy-start.33
  181.6 1.7 copy-start.34
  181.6 1.7 copy-start.35
  183.2 1.9 copy-start.19
  210.9 5.6 %copy-start.13 = (f32[3,128,2,8]{1,3,2,0:T(8,128)S(1)}, f32[3,128,2,8]{1,3,2,0:T(8,128)}, u32[]{:S(2)}) copy-start(f32[3,128,2,8]{1,3,2,0:T(8,128)} %copy.142) | copy-start | bytes 73732
  210.9 5.6 %copy-start.42 = (f32[3,2,8]{2,1,0:T(2,128)S(1)}, f32[3,2,8]{2,1,0:T(2,128)}, u32[]{:S(2)}) copy-start(f32[3,2,8]{2,1,0:T(2,128)} %fusion.21) | copy-start | bytes 580
  231.6 2.1 copy-start.2
  231.6 2.9 %copy-start.43 = (bf16[4096]{0:T(1024)(128)(2,1)S(1)}, bf16[4096]{0:T(1024)(128)(2,1)}, u32[]{:S(2)}) copy-start(bf16[4096]{0:T(1024)(128)(2,1)} %param.39) | copy-start | bytes 24580
  233.7 4.1 %collective-permute-start.1 = (bf16[384,2048]{1,0:T(8,128)(2,1)}, bf16[384,2048]{1,0:T(8,128)(2,1)S(1)}, u32[]{:S(2)}, u32[]{:S(2)}) collective-permute-start(bf16[384,2048]{1,0:T(8,128)(2,1)} %constant_dynamic-slice_fusion), channel_id=1, source_target_pairs={{0,1},{1,0},{2,3},{3,2},{4,5},{5,4},{6,7},{7,6},{8,9},{9,8},{10,11... | collective-permute-start | bytes 4718600 | tf_op jit(solution)/shard_map/ppermute | solution.py:415
  (3 other events, 3.4 us)
Sparse Core Ops, SparseCore 0:
  180.2 30.6 all-gather.4

commit v2 on v0

v2 whole, which is shorter than its diff:
```python
import functools

import jax
import jax.numpy as jnp
from jax import lax
from jax.experimental import pallas as pl
from jax.experimental.pallas import tpu as pltpu
from jax.sharding import PartitionSpec as P

D = 4096
HEAD_DIM = 64
STATE = 128
CONV = 4
BLOCK = 128
POOL_GROUPS = 4
POOL_GROUP = 256


eps = 1e-06


def passed_along(block, axis, distance):
    devices = range(lax.axis_size(axis))
    route = [(i - distance, i) for i in devices if i - distance in devices]
    return lax.ppermute(block, axis, route)


def entering_2(array, axis, join, neutral):
    place = lax.axis_index(axis)
    gathered = jax.tree.map(
        lambda a, kind: lax.all_gather(a.astype(kind), axis), array, (jnp.bfloat16, jnp.bfloat16)
    )
    state = jax.tree.map(lambda a, e: jnp.zeros_like(a) + jnp.asarray(e, a.dtype), array, neutral)

    def one(lap, state):
        return join(
            state,
            jax.tree.map(
                lambda a, own: lax.dynamic_index_in_dim(a, lap, 0, False).astype(own.dtype),
                gathered,
                array,
            ),
        )

    return lax.fori_loop(0, place, one, state)


MESH_IDS = pl.DeviceIdType.MESH
EXACT = lax.Precision.HIGHEST


def ring_place(index, size):
    if size != 4:
        return index
    return index + (index // 2) * (1 - 2 * (index % 2))


class Gather:
    def __init__(self, own, whole, sends, arrivals, sp_size, fs_size):
        self.own, self.whole = own, whole
        self.sends, self.arrivals = sends, arrivals
        self.width = own.shape[1]
        self.sp_size, self.fs_size = sp_size, fs_size
        self.sp_me = lax.axis_index("sp")
        self.fs_me = ring_place(lax.axis_index("fs"), fs_size)
        rows = own.shape[0]
        self.cut = rows * 3 // 4 // 64 * 64
        self.keys = {}
        self.fs_last = fs_size // 2
        self.fs_offsets = [0]
        for step in range(1, self.fs_last + 1):
            self.fs_offsets.append(-step)
            if not self.halved(step):
                self.fs_offsets.append(step)

    def halved(self, step):
        return self.fs_size % 2 == 0 and step == self.fs_last

    def fs_at(self, offset):
        return ring_place(lax.rem(self.fs_me + offset + 2 * self.fs_size, self.fs_size), self.fs_size)

    def copy(self, part, stage, cross, step, way):
        on_sp = part == stage
        low, high = (0, self.cut) if part == 0 else (self.cut, self.own.shape[0])
        if not on_sp and self.halved(step):
            mid = low + (high - low) // 2
            low, high = (low, mid) if way == 1 else (mid, high)
        rows = pl.ds(low, high - low)
        off = -way * (step - 1)
        sp_off, fs_off = (off, cross) if on_sp else (cross, off)
        at = ((self.sp_me + sp_off) * self.fs_size + self.fs_at(fs_off)) * self.width
        cols = pl.ds(pl.multiple_of(at, self.width), self.width)
        first = sp_off == 0 and fs_off == 0
        spot = self.keys.setdefault((part, stage, cross, step, way), len(self.keys))
        return pltpu.make_async_remote_copy(
            src_ref=self.own.at[rows] if first else self.whole.at[rows, cols],
            dst_ref=self.whole.at[rows, cols],
            send_sem=self.sends.at[spot],
            recv_sem=self.arrivals.at[spot],
            device_id={"sp": self.sp_me + way} if on_sp else {"fs": self.fs_at(way)},
            device_id_type=MESH_IDS,
        )

    def when(self, part, stage, cross, step, way, arriving):
        if part == stage:
            gone = step if arriving else step - 1
            origin = self.sp_me - way * gone
            far = self.sp_me if arriving else self.sp_me + way
            checks = [origin >= 0, origin < self.sp_size, far >= 0, far < self.sp_size]
        elif cross:
            checks = [self.sp_me + cross >= 0, self.sp_me + cross < self.sp_size]
        else:
            return None
        return functools.reduce(jnp.logical_and, checks)

    def each(self, part, stage, cross, step, arriving, act):
        last = self.sp_size - 1 if part == stage else self.fs_last
        if not 1 <= step <= last:
            return
        for way in (1, -1):
            key = (part, stage, cross, step, way)
            here = self.when(*key, arriving)

            def run(key=key):
                act(self.copy(*key))

            if here is None:
                run()
            else:
                pl.when(here)(run)

    def send(self, *key):
        self.each(*key, False, lambda copy: copy.start())

    def take(self, *key):
        self.each(*key, True, lambda copy: copy.wait_recv())

    def barrier(self):
        barrier = pltpu.get_barrier_semaphore()
        total = 0
        for far in range(1, self.sp_size):
            other = lax.rem(self.sp_me + far, self.sp_size)
            pl.semaphore_signal(barrier, inc=1, device_id={"sp": other}, device_id_type=MESH_IDS)
            total += 1
        if self.fs_size > 1:
            for way in (1, -1):
                other = self.fs_at(way)
                pl.semaphore_signal(
                    barrier, inc=1, device_id={"fs": other}, device_id_type=MESH_IDS
                )
                total += 1
        if total:
            pl.semaphore_wait(barrier, total)

    def pair(self, off):
        return [0] if off == 0 else [-off, off]

    def run(self):
        rounds = max(self.sp_size - 1, self.fs_last)
        self.send(0, 0, 0, 1)
        self.send(1, 0, 0, 1)
        self.send(0, 1, 0, 1)
        for step in range(1, rounds + 1):
            yield
            self.take(0, 0, 0, step)
            self.send(0, 0, 0, step + 1)
            if step < self.sp_size:
                for cross in self.pair(step):
                    self.send(0, 1, cross, 1)
            if step == 1:
                self.send(1, 1, 0, 1)
            self.take(1, 0, 0, step)
            self.send(1, 0, 0, step + 1)
            for cross in self.fs_offsets[1:]:
                if abs(cross) == step:
                    self.send(1, 1, cross, 1)
            yield
            if step <= self.sp_size:
                for cross in self.pair(step - 1):
                    self.take(0, 1, cross, 1)
                    self.send(0, 1, cross, 2)
            yield
            if step > self.fs_last:
                for cross in self.fs_offsets:
                    self.take(1, 1, cross, step - self.fs_last)
                    self.send(1, 1, cross, step - self.fs_last + 1)
        for late in range(rounds, self.sp_size):
            yield
            for cross in self.pair(late):
                self.take(0, 1, cross, 1)
                self.send(0, 1, cross, 2)
        for step in range(max(rounds - self.fs_last, 0) + 1, self.sp_size):
            for cross in self.fs_offsets:
                yield
                self.take(1, 1, cross, step)
                self.send(1, 1, cross, step + 1)
        for step in range(2, self.fs_last + 1):
            for off in range(self.sp_size):
                yield
                for cross in self.pair(off):
                    self.take(0, 1, cross, step)
                    self.send(0, 1, cross, step + 1)

    def finish(self):
        for key in list(self.keys):
            part, stage, cross, step, way = key
            here = self.when(*key, False)

            def run(key=key):
                self.copy(*key).wait_send()

            if here is None:
                run()
            else:
                pl.when(here)(run)


def hop_count(sp_size, fs_size):
    along, around = 2 * (sp_size - 1), 2 * (fs_size // 2)
    return along * (1 + fs_size) + around * (1 + 2 * sp_size - 1)


def silu(rows):
    return rows / (1.0 + jnp.exp(-rows))


def softplus(rows):
    return jnp.maximum(rows, 0.0) + jnp.log(1.0 + jnp.exp(-jnp.abs(rows)))


def mixers(sizes, refs, links):
    sp_size, tail = sizes
    (x_in, gate, bc_in, dt, dt_t, added, added_t, rates, rates_t, x_taps, bc_taps, bc_bias, gain,
     pool_in, pool_weight, pool_scale, reach, prior, channels, x_pad, bc_pad, pool_pad, x_conv,
     bc_conv, within, grown, local_in, state, ends, before, far_state, far_log) = refs
    sends, arrivals = links
    rows, inner = x_in.shape
    heads = dt.shape[1]
    wide = bc_in.shape[1] // 2
    groups = wide // STATE
    span = inner // groups
    blocks = rows // BLOCK
    sp_me = lax.axis_index("sp")
    x_pad[0:tail] = prior[:, 0:inner].astype(jnp.float32)
    bc_pad[0:tail] = prior[:, inner : inner + 2 * wide].astype(jnp.float32)
    pool_pad[0:tail] = prior[:, inner + 2 * wide :].astype(jnp.float32)
    x_pad[tail:] = x_in[...].astype(jnp.float32)
    bc_pad[tail:] = bc_in[...].astype(jnp.float32)
    pool_pad[tail:] = pool_in[...].astype(jnp.float32)
    step_all = softplus(dt[...].astype(jnp.float32))
    log_all = -step_all * jnp.exp(rates[...]) + added[...]
    step_flat = softplus(dt_t[...].astype(jnp.float32))
    log_flat = -step_flat * jnp.exp(rates_t[...]) + added_t[...]
    down = lax.broadcasted_iota(jnp.int32, (BLOCK, BLOCK), 0)
    across = lax.broadcasted_iota(jnp.int32, (BLOCK, BLOCK), 1)
    causal = down >= across
    lower = causal.astype(jnp.float32)
    upper = (down <= across).astype(jnp.float32)
    first_half = lax.broadcasted_iota(jnp.int32, (BLOCK, 2 * HEAD_DIM), 1) < HEAD_DIM
    yield

    def taps(pad, weights, at, cols):
        total = None
        for tap in range(CONV):
            begin = at * BLOCK + tail - CONV + 1 + tap
            term = pad[begin : begin + BLOCK, cols] * weights[tap : tap + 1, cols].astype(
                jnp.float32
            )
            total = term if total is None else total + term
        return total

    state[...] = jnp.zeros_like(state)
    for at in range(blocks):
        now = slice(at * BLOCK, (at + 1) * BLOCK)
        every = slice(0, 2 * wide)
        bc_conv[now] = silu(
            taps(bc_pad, bc_taps, at, every) + bc_bias[...].astype(jnp.float32)
        ).astype(jnp.bfloat16)
        cum = jnp.dot(lower, log_all[now], precision=EXACT, preferred_element_type=jnp.float32)
        cum_flat = jnp.dot(
            log_flat[:, now], upper, precision=EXACT, preferred_element_type=jnp.float32
        )
        step_row = step_flat[:, now]
        for group in range(groups):
            cols = slice(group * span, (group + 1) * span)
            x_now = silu(taps(x_pad, x_taps, at, cols))
            x_half = x_now.astype(jnp.bfloat16)
            b_now = bc_conv[now, group * STATE : (group + 1) * STATE]
            c_now = bc_conv[now, wide + group * STATE : wide + (group + 1) * STATE]
            spread = (
                lax.broadcasted_iota(jnp.int32, (heads, span), 0)
                == group * (span // HEAD_DIM)
                + lax.broadcasted_iota(jnp.int32, (heads, span), 1) // HEAD_DIM
            ).astype(jnp.float32)
            cum_wide = jnp.dot(cum, spread, precision=EXACT, preferred_element_type=jnp.float32)
            step_wide = jnp.dot(
                step_all[now], spread, precision=EXACT, preferred_element_type=jnp.float32
            )
            grown[now, cols] = jnp.exp(cum_wide)
            end = cum_wide[BLOCK - 1 : BLOCK]
            ends[at : at + 1, cols] = end
            scaled = (x_half.astype(jnp.float32) * jnp.exp(end - cum_wide) * step_wide).astype(
                jnp.bfloat16
            )
            b_flat = jnp.transpose(b_now.astype(jnp.float32)).astype(jnp.bfloat16)
            local_in[at, :, cols] = state[:, cols]
            state[:, cols] = state[:, cols] * jnp.exp(end) + jnp.dot(
                b_flat, scaled, preferred_element_type=jnp.float32
            )
            scores = jnp.dot(c_now, b_flat, preferred_element_type=jnp.float32)
            for pair in range(span // (2 * HEAD_DIM)):
                lanes = slice(pair * 2 * HEAD_DIM, (pair + 1) * 2 * HEAD_DIM)
                both = []
                for side in range(2):
                    head = group * (span // HEAD_DIM) + 2 * pair + side
                    gap = cum[:, head : head + 1] - cum_flat[head : head + 1]
                    decay = jnp.exp(jnp.where(causal, gap, -1e30))
                    weights = (scores * decay * step_row[head : head + 1]).astype(jnp.bfloat16)
                    both.append(
                        jnp.dot(weights, x_half[:, lanes], preferred_element_type=jnp.float32)
                    )
                here = group * span + pair * 2 * HEAD_DIM
                within[now, here : here + 2 * HEAD_DIM] = jnp.where(first_half, both[0], both[1])
            yield
    total_log = ends[0:1]
    for at in range(1, blocks):
        total_log = total_log + ends[at : at + 1]
    far_state[sp_size] = state[...].astype(jnp.bfloat16)
    far_log[sp_size] = jnp.broadcast_to(total_log, far_log.shape[1:])

    def letters(far):
        return [
            pltpu.make_async_remote_copy(
                src_ref=buffer.at[sp_size],
                dst_ref=buffer.at[far - 1],
                send_sem=sends.at[far - 1, kind],
                recv_sem=arrivals.at[far - 1, kind],
                device_id={"sp": sp_me + far},
                device_id_type=MESH_IDS,
            )
            for kind, buffer in enumerate((far_state, far_log))
        ]

    for far in range(1, sp_size):

        @pl.when(sp_me + far < sp_size)
        def _(far=far):
            for letter in letters(far):
                letter.start()

    yield
    place = sp_me * rows
    for group in range(pool_weight.shape[0]):
        cols = slice(group * POOL_GROUP, (group + 1) * POOL_GROUP)
        window = reach[:, cols]
        for at in range(blocks):
            now = slice(at * BLOCK, (at + 1) * BLOCK)
            running = None
            for back in range(tail):
                begin = at * BLOCK + tail - back
                term = pool_pad[begin : begin + BLOCK, cols] * jnp.where(back < window, 1.0, 0.0)
                running = term if running is None else running + term
            position = (
                place + at * BLOCK + lax.broadcasted_iota(jnp.int32, (BLOCK, POOL_GROUP), 0)
            ).astype(jnp.float32)
            pooled = running / jnp.minimum(position + 1.0, window) - pool_in[now, cols].astype(
                jnp.float32
            )
            mixed = jnp.dot(
                pooled.astype(jnp.bfloat16), pool_weight[group], preferred_element_type=jnp.float32
            )
            out = inner + group * POOL_GROUP
            channels[now, out : out + POOL_GROUP] = (
                mixed * pool_scale[:, cols].astype(jnp.float32)
            ).astype(jnp.bfloat16)
        yield
    before[...] = jnp.zeros_like(before)
    for far in range(sp_size - 1, 0, -1):

        @pl.when(sp_me - far >= 0)
        def _(far=far):
            for letter in letters(far):
                letter.wait_recv()
            before[...] = before[...] * jnp.exp(far_log[far - 1][0:1]) + far_state[far - 1].astype(
                jnp.float32
            )

    yield
    prefix = jnp.zeros_like(total_log)
    for at in range(blocks):
        now = slice(at * BLOCK, (at + 1) * BLOCK)
        for group in range(groups):
            cols = slice(group * span, (group + 1) * span)
            entering = local_in[at, :, cols] + jnp.exp(prefix[:, cols]) * before[:, cols]
            c_now = bc_conv[now, wide + group * STATE : wide + (group + 1) * STATE]
            carried = jnp.dot(
                c_now, entering.astype(jnp.bfloat16), preferred_element_type=jnp.float32
            )
            mixed = (within[now, cols] + carried * grown[now, cols]) * silu(
                gate[now, cols].astype(jnp.float32)
            )
            root = lax.rsqrt(jnp.mean(mixed * mixed, axis=1, keepdims=True) + eps)
            channels[now, cols] = (mixed * root * gain[:, cols].astype(jnp.float32)).astype(
                jnp.bfloat16
            )
        prefix = prefix + ends[at : at + 1]
        yield
    for far in range(1, sp_size):

        @pl.when(sp_me + far < sp_size)
        def _(far=far):
            for letter in letters(far):
                letter.wait_send()


def whole_kernel(sp_size, fs_size, tail, own, *refs):
    inputs, (whole, channels), scratch = refs[:18], refs[18:20], refs[20:]
    sends, arrivals, local_sem, letter_sends, letter_arrivals = scratch[:5]
    gather = Gather(own, whole, sends, arrivals, sp_size, fs_size)
    gather.barrier()
    at = (gather.sp_me * fs_size + gather.fs_at(0)) * gather.width
    mine = pltpu.make_async_copy(
        own, whole.at[:, pl.ds(pl.multiple_of(at, gather.width), gather.width)], local_sem
    )
    mine.start()
    moves = gather.run()
    work = mixers(
        (sp_size, tail), (*inputs, channels, *scratch[5:]), (letter_sends, letter_arrivals)
    )
    next(moves, None)
    for _ in work:
        next(moves, None)
    for _ in moves:
        pass
    mine.wait()
    gather.finish()


def mixed_and_gathered(own, inputs, tail):
    sp_size, fs_size = lax.axis_size("sp"), lax.axis_size("fs")
    rows, width = own.shape
    x_in, bc_in, pool_in = inputs[0], inputs[2], inputs[13]
    tok_rows, inner = x_in.shape
    blocks = tok_rows // BLOCK
    hops = hop_count(sp_size, fs_size)
    vmem = pl.BlockSpec(memory_space=pltpu.VMEM)
    return pl.pallas_call(
        functools.partial(whole_kernel, sp_size, fs_size, tail),
        out_shape=(
            jax.ShapeDtypeStruct((rows, width * sp_size * fs_size), own.dtype),
            jax.ShapeDtypeStruct((tok_rows, inner + pool_in.shape[1]), jnp.bfloat16),
        ),
        in_specs=[vmem] * (1 + len(inputs)),
        out_specs=(vmem, vmem),
        scratch_shapes=[
            pltpu.SemaphoreType.DMA((hops,)),
            pltpu.SemaphoreType.DMA((hops,)),
            pltpu.SemaphoreType.DMA,
            pltpu.SemaphoreType.DMA((sp_size, 2)),
            pltpu.SemaphoreType.DMA((sp_size, 2)),
            pltpu.VMEM((tail + tok_rows, inner), jnp.float32),
            pltpu.VMEM((tail + tok_rows, bc_in.shape[1]), jnp.float32),
            pltpu.VMEM((tail + tok_rows, pool_in.shape[1]), jnp.float32),
            pltpu.VMEM((8, 128), jnp.bfloat16),
            pltpu.VMEM((tok_rows, bc_in.shape[1]), jnp.bfloat16),
            pltpu.VMEM((tok_rows, inner), jnp.float32),
            pltpu.VMEM((tok_rows, inner), jnp.float32),
            pltpu.VMEM((blocks, STATE, inner), jnp.float32),
            pltpu.VMEM((STATE, inner), jnp.float32),
            pltpu.VMEM((-(-blocks // 8) * 8, inner), jnp.float32),
            pltpu.VMEM((STATE, inner), jnp.float32),
            pltpu.VMEM((sp_size + 1, STATE, inner), jnp.bfloat16),
            pltpu.VMEM((sp_size + 1, 8, inner), jnp.float32),
        ],
        compiler_params=pltpu.CompilerParams(
            collective_id=0, has_side_effects=True, vmem_limit_bytes=48 * 2**20
        ),
        name="mega_mixers",
    )(own, *inputs)


def causal_taps(input_rows, prior_rows, tap_weights, offset_bias):
    padded = jnp.concatenate([prior_rows, input_rows], axis=0).astype(jnp.float32)
    tok_rows = input_rows.shape[0]
    running = jnp.zeros(input_rows.shape, jnp.float32) + offset_bias
    for tap_index in range(tap_weights.shape[0]):
        running = (
            running
            + tap_weights[tap_index].astype(jnp.float32) * padded[tap_index : tap_index + tok_rows]
        )
    return jax.nn.silu(running).astype(jnp.bfloat16)


def pool_mix(input_rows, prior_rows, positions, group_ids, local_weight, local_scale):
    tail_rows = prior_rows.shape[0]
    tok_rows = input_rows.shape[0]
    padded = jnp.concatenate([prior_rows, input_rows], axis=0).astype(jnp.float32)
    window_reach = jnp.left_shift(jnp.int32(2), group_ids)
    running = jnp.zeros(input_rows.shape, jnp.float32)
    for offset_back in range(tail_rows + 1):
        start_row = tail_rows - offset_back
        running = running + padded[start_row : start_row + tok_rows] * (
            offset_back < window_reach
        ).astype(jnp.float32)
    window_count = jnp.minimum(positions[:, None] + 1.0, window_reach.astype(jnp.float32)[None, :])
    pooled = (running / window_count - input_rows.astype(jnp.float32)).astype(jnp.bfloat16)
    grouped = pooled.reshape(tok_rows, local_weight.shape[0], local_weight.shape[1])
    mixed = jnp.einsum("lgc,gcd->lgd", grouped, local_weight, preferred_element_type=jnp.float32)
    return (mixed.reshape(input_rows.shape) * local_scale.astype(jnp.float32)).astype(jnp.bfloat16)


def join_states(earlier, later_part):
    return (
        earlier[0] + later_part[0],
        earlier[1] * jnp.exp(later_part[0])[..., None, None] + later_part[1],
    )


def body(
    statespace_input,
    output_gate_input,
    state_input_projection,
    state_output_projection,
    step_size_input,
    added_log_decay,
    logarithm_rates,
    head_channel_taps,
    input_projection_taps,
    output_projection_taps,
    input_projection_bias,
    group_norm_gain,
    pooling_input,
    pooling_group_weight,
    pooling_channel_scale,
    statespace_output_weight,
    pooling_output_weight,
    output_norm_gain,
):
    core_index = lax.axis_index("tp")
    core_count = lax.axis_size("tp")
    seq_index = lax.axis_index("sp")
    head_channel_rows = statespace_input[0]
    output_gate_rows = output_gate_input[0]
    input_projection_rows = state_input_projection[0]
    output_projection_rows = state_output_projection[0]
    step_size_rows = step_size_input[0]
    decay_spikes = added_log_decay[0]
    pooling_rows = pooling_input[0]
    tok_rows = head_channel_rows.shape[0]
    inner_local = head_channel_rows.shape[1]
    heads_local = step_size_rows.shape[1]
    state_local = input_projection_rows.shape[1]
    pool_local = pooling_rows.shape[1]
    groups_local = state_local // STATE
    per_group = heads_local // groups_local
    groups_pool = pool_local // POOL_GROUP
    pool_tail = 2**POOL_GROUPS - 1
    conv_tail = CONV - 1
    own_columns = jnp.concatenate([statespace_output_weight, pooling_output_weight], axis=0)
    tails = jnp.concatenate(
        [
            jnp.pad(rows[tok_rows - tail :], ((pool_tail - tail, 0), (0, 0)))
            for rows, tail in (
                (head_channel_rows, conv_tail),
                (input_projection_rows, conv_tail),
                (output_projection_rows, conv_tail),
                (pooling_rows, pool_tail),
            )
        ],
        axis=1,
    )
    prior = passed_along(tails, "sp", 1)
    widths = (inner_local, state_local, state_local, pool_local)
    prior_x, prior_b, prior_c, prior_pool = (
        prior[pool_tail - tail :, sum(widths[:at]) : sum(widths[: at + 1])]
        for at, tail in enumerate((conv_tail, conv_tail, conv_tail, pool_tail))
    )
    taps_x = lax.dynamic_slice_in_dim(head_channel_taps, core_index * inner_local, inner_local, 1)
    taps_b = lax.dynamic_slice_in_dim(
        input_projection_taps, core_index * state_local, state_local, 1
    )
    taps_c = lax.dynamic_slice_in_dim(
        output_projection_taps, core_index * state_local, state_local, 1
    )
    bias_b = lax.dynamic_slice_in_dim(
        input_projection_bias, core_index * state_local, state_local, 0
    )
    gain_ssd = lax.dynamic_slice_in_dim(group_norm_gain, core_index * inner_local, inner_local, 0)
    head_decay_rates = jnp.exp(
        lax.dynamic_slice_in_dim(logarithm_rates, core_index * heads_local, heads_local, 0)
    )
    gain_pool = lax.dynamic_slice_in_dim(
        pooling_channel_scale, core_index * pool_local, pool_local, 0
    )
    weight_pool = lax.dynamic_slice_in_dim(
        pooling_group_weight, core_index * groups_pool, groups_pool, 0
    )
    tail = pool_tail + 1
    local_width = own_columns.shape[1]
    narrow = local_width % 128 != 0 or lax.axis_size("sp") > 8
    if narrow:
        whole_columns = lax.all_gather(own_columns, ("sp", "fs"), axis=1, tiled=True)
        x_conv = causal_taps(head_channel_rows, prior_x, taps_x, 0.0)
        b_conv = causal_taps(input_projection_rows, prior_b, taps_b, bias_b.astype(jnp.float32))
        c_conv = causal_taps(output_projection_rows, prior_c, taps_c, 0.0)
        blocks = tok_rows // BLOCK
        discrete_step_size = jax.nn.softplus(step_size_rows.astype(jnp.float32))
        logarithm_decay = -discrete_step_size * head_decay_rates + decay_spikes
        cumulative_decay = jnp.cumsum(
            logarithm_decay.reshape(blocks, BLOCK, groups_local, per_group), axis=1
        )
        cum_t = cumulative_decay.transpose(0, 2, 3, 1)
        step_t = discrete_step_size.reshape(blocks, BLOCK, groups_local, per_group).transpose(
            0, 2, 3, 1
        )
        heads_x = x_conv.reshape(blocks, BLOCK, groups_local, per_group, HEAD_DIM)
        group_b = b_conv.reshape(blocks, BLOCK, groups_local, STATE)
        group_c = c_conv.reshape(blocks, BLOCK, groups_local, STATE)
        scores = jnp.einsum("ktgn,kugn->kgtu", group_c, group_b, preferred_element_type=jnp.float32)
        causal = jnp.arange(BLOCK)[:, None] >= jnp.arange(BLOCK)[None, :]
        decay_gap = cum_t[..., :, None] - cum_t[..., None, :]
        decay_factor = jnp.where(causal, jnp.exp(jnp.where(causal, decay_gap, 0.0)), 0.0)
        weights = (scores[:, :, None] * decay_factor * step_t[..., None, :]).astype(jnp.bfloat16)
        within = jnp.einsum("kgetu,kugep->ktgep", weights, heads_x, preferred_element_type=jnp.float32)
        block_end = cum_t[..., -1]
        end_weight = jnp.exp(block_end[..., None] - cum_t) * step_t
        scaled_x = (heads_x * end_weight.transpose(0, 3, 1, 2)[..., None]).astype(jnp.bfloat16)
        block_state = jnp.einsum(
            "kugep,kugn->kgepn", scaled_x, group_b, preferred_element_type=jnp.float32
        )

        def local_chain(state_now, current_inputs):
            piece_state, piece_fall = current_inputs
            return (state_now * jnp.exp(piece_fall)[..., None, None] + piece_state, state_now)

        final_state, local_entering = lax.scan(
            local_chain, jnp.zeros(block_state.shape[1:], jnp.float32), (block_state, block_end)
        )
        log_total = jnp.sum(block_end, axis=0)
        prefix_log = jnp.cumsum(block_end, axis=0) - block_end
        log_before, state_before = entering_2(
            (log_total, final_state),
            "sp",
            join_states,
            (jnp.zeros_like(log_total), jnp.zeros_like(final_state)),
        )
        entering = (local_entering + jnp.exp(prefix_log)[..., None, None] * state_before[None]).astype(
            jnp.bfloat16
        )
        carried_out = jnp.einsum(
            "ktgn,kgepn->ktgep", group_c, entering, preferred_element_type=jnp.float32
        )
        carried_out = carried_out * jnp.exp(cumulative_decay)[..., None]
        mixed_ssd = (within + carried_out).reshape(tok_rows, inner_local) * jax.nn.silu(
            output_gate_rows.astype(jnp.float32)
        )
        grouped = mixed_ssd.reshape(tok_rows, groups_local, inner_local // groups_local)
        normed = grouped * lax.rsqrt(jnp.mean(grouped * grouped, axis=-1, keepdims=True) + eps)
        ssd_out = (normed.reshape(tok_rows, inner_local) * gain_ssd.astype(jnp.float32)).astype(
            jnp.bfloat16
        )
        positions = (seq_index * tok_rows + jnp.arange(tok_rows, dtype=jnp.int32)).astype(jnp.float32)
        group_ids = core_index * groups_pool + jnp.arange(pool_local, dtype=jnp.int32) // POOL_GROUP
        pool_out = pool_mix(pooling_rows, prior_pool, positions, group_ids, weight_pool, gain_pool)
        channels = jnp.concatenate([ssd_out, pool_out], axis=1)
    else:
        rates = lax.dynamic_slice_in_dim(logarithm_rates, core_index * heads_local, heads_local, 0)
        group_ids = core_index * groups_pool + jnp.arange(pool_local, dtype=jnp.int32) // POOL_GROUP
        reach = jnp.left_shift(jnp.int32(2), group_ids).astype(jnp.float32)
        bias = jnp.concatenate([bias_b, jnp.zeros_like(bias_b)])
        whole_columns, channels = mixed_and_gathered(
            own_columns,
            (
                head_channel_rows,
                output_gate_rows,
                jnp.concatenate([input_projection_rows, output_projection_rows], axis=1),
                step_size_rows,
                step_size_rows.T,
                decay_spikes,
                decay_spikes.T,
                rates[None],
                rates[:, None],
                taps_x,
                jnp.concatenate([taps_b, taps_c], axis=1),
                bias[None],
                gain_ssd[None],
                pooling_rows,
                weight_pool,
                gain_pool[None],
                reach[None],
                jnp.pad(prior, ((tail - pool_tail, 0), (0, 0))),
            ),
            tail,
        )
    half_width = D // core_count
    gain_out = lax.dynamic_slice_in_dim(
        output_norm_gain, core_index * half_width, half_width, 0
    ).astype(jnp.float32)
    partial = jnp.dot(channels, whole_columns, preferred_element_type=jnp.float32).astype(
        jnp.bfloat16
    )
    own_half = lax.dynamic_slice_in_dim(partial, core_index * half_width, half_width, 1).astype(
        jnp.float32
    )
    for hop in range(1, core_count):
        target = lax.rem(core_index + hop, core_count)
        leaving = lax.dynamic_slice_in_dim(partial, target * half_width, half_width, 1)
        route = [(i, (i + hop) % core_count) for i in range(core_count)]
        own_half = own_half + lax.ppermute(leaving, "tp", route).astype(jnp.float32)
    row_squares = lax.psum(jnp.sum(own_half * own_half, axis=1), "tp")
    result = own_half * lax.rsqrt(row_squares / D + eps)[:, None] * gain_out
    return result.astype(jnp.bfloat16)[None]


def solution(mesh):
    in_specs = (
        P("fs", "sp", "tp"),
        P("fs", "sp", "tp"),
        P("fs", "sp", "tp"),
        P("fs", "sp", "tp"),
        P("fs", "sp", "tp"),
        P("fs", "sp", "tp"),
        P(),
        P(),
        P(),
        P(),
        P(),
        P(),
        P("fs", "sp", "tp"),
        P(),
        P(),
        P("tp", ("sp", "fs")),
        P("tp", ("sp", "fs")),
        P(),
    )
    out_specs = P("fs", "sp", "tp")
    return jax.shard_map(body, mesh=mesh, in_specs=in_specs, out_specs=out_specs, check_vma=False)
```

time: 293 us -> 158 us (0.54)
  waiting for transfers between devices: 184 us -> 3.24 us
  Pallas kernels: 0 us -> 117 us
  starting transfers between devices: 20 us -> 3.33 us
  matrix products: 24.4 us -> 9.84 us
  between operations: 13.8 us -> 0.18 us
  other arithmetic: 20.5 us -> 8.26 us
  blocking collectives: 14 us -> 2.49 us
    all_gather x4 -> x0, waiting for transfers between devices: 180 us -> none  [the longest x1 99.9 us: body(): lax.all_gather(statespace_output_weight, ('sp', 'fs'), axis=1, tiled=True)]
    pallas_call x0 -> x1, Pallas kernels: none -> 117 us  [mixed_and_gathered(): pl.pallas_call(functools.partial(whole_kernel, sp_size, fs_size, tail), o...]
    all_to_all x2 -> x0, starting transfers between devices: 14.7 us -> none  [the longest x1 7.64 us: body(): lax.all_to_all(whole_ssd, 'tp', split_axis=1, concat_axis=0, tiled=True)]
    dot_general x9 -> x1, matrix products: 24.4 us -> 9.84 us  [body(): jnp.dot(channels, whole_columns, preferred_element_type=jnp.float32)]
    all_gather x2 -> x0, blocking collectives: 11.5 us -> none  [the longest x1 8.99 us: entering_2(): lax.all_gather(a.astype(kind), axis)]
    convert_element_type x24 -> x1, other arithmetic: 8.61 us -> 0.01 us  [body(): reach = jnp.left_shift(jnp.int32(2), group_ids).astype(jnp.float32)]
    dynamic_slice x0 -> x7, local copies, waits for them, and re-layouts: none -> 4.95 us  [the longest x1 1.32 us: body(): lax.dynamic_slice_in_dim(partial, target * half_width, half_width, 1)]
    ppermute x4 -> x1, waiting for transfers between devices: 4.1 us -> 0.01 us  [passed_along(): return lax.ppermute(block, axis, route)]
  transfers between devices with their start and end apart: 10 -> 2, of which waited for: 5 -> 1; matrix products, arithmetic and copies ran while one was open for 10% -> 5% of each run, Pallas kernels for 0% -> 0%
where the time goes in v2:
time: 158 us
  Pallas kernels  117 us (74%)
  local copies, waits for them, and re-layouts  13.4 us (8%)
  matrix products  9.84 us (6%)
  other arithmetic  8.26 us (5%)
  starting transfers between devices  3.33 us (2%)
  waiting for transfers between devices  3.24 us (2%)
  blocking collectives  2.49 us (2%)
    pallas_call x1, Pallas kernels, mixed_and_gathered(): pl.pallas_call(functools.partial(whole_kernel, sp_size, fs_size, tail), o...  117 us
    dot_general x1, matrix products, body(): jnp.dot(channels, whole_columns, preferred_element_type=jnp.float32)  9.84 us
    broadcast_in_dim x1, other arithmetic, body(): return result.astype(jnp.bfloat16)[None]  3.36 us
    ppermute x1, waiting for transfers between devices, body(): own_half = own_half + lax.ppermute(leaving, 'tp', route).astype(jnp.float32)  3.24 us
  transfers between devices with their start and end apart: 2, of which 1 were waited for; matrix products, arithmetic and copies ran while one was open for 5% of the time, Pallas kernels for 0%

profile of v2, /device:TPU:25, one launch (start us, length us, event | category | flops | bytes accessed | tf_op | source)
XLA Modules:
  0.0 157.5 jit_solution(12189237874491325144)
XLA Ops:
  0.0 0.0 copy-start
  0.0 0.0 copy-start.3
  0.0 0.0 copy-start.1
  0.0 0.0 copy-start.4
  0.0 0.0 copy-start.5
  0.0 0.8 slice_bitcast_fusion
  0.9 0.7 slice_bitcast_fusion.1
  1.6 0.7 slice_bitcast_fusion.2
  2.3 0.6 fusion.7
  3.0 1.3 collective-permute-start
  4.3 0.7 dynamic-slice_bitcast_fusion
  5.0 0.1 copy.21.refs_8_
  5.1 0.7 constant_dynamic-slice_fusion.4.refs_9_
  5.8 0.7 dynamic_slice.38
  6.5 0.8 dynamic_slice.37
  7.2 0.8 dynamic_slice.40
  8.0 0.9 copy.20.refs_5_
  8.9 0.8 copy.19.refs_3_
  9.7 0.7 constant_dynamic-slice_fusion.2
  10.4 0.0 copy-done
  10.5 1.2 pad_maximum_fusion.own
  11.6 1.1 pad_maximum_fusion.1.refs_2_
  12.7 0.0 collective-permute-done
  12.7 0.9 pad.19.refs_17_
  13.6 0.0 copy-done.3
  13.6 0.0 copy-done.1
  13.6 0.0 copy-done.4
  13.6 0.0 copy-done.5
  13.6 0.0 copy-start.2
  13.7 1.1 copy-done.2
  14.8 116.8 %mega_mixers.1 = (bf16[1536,4096]{1,0:T(8,128)(2,1)}, bf16[384,1536]{1,0:T(8,128)(2,1)S(1)}) custom-call(bf16[1536,256]{1,0:T(8,128)(2,1)S(1)} %pad_maximum_fusion.own, bf16[384,1024]{1,0:T(8,128)(2,1)S(1)} %bitcast.27, bf16[384,1024]{1,0:T(8,128)(2,1)S(1)} %bitcast.28, bf16[384,512]{1,0:T(8,128)(2,1)S(1)} %pad_maximum_fusion.1.refs_2_, ...), custom_call_target="tpu_custom_call" | custom-call | tf_op jit(solution)/shard_map/mega_mixers/pallas_call | solution.py:447
  131.6 9.8 %convolution_convert_fusion = bf16[384,4096]{1,0:T(8,128)(2,1)S(1)} fusion(bf16[384,1536]{1,0:T(8,128)(2,1)S(1)} %get-tuple-element.7, bf16[1536,4096]{1,0:T(8,128)(2,1)} %get-tuple-element.8), kind=kOutput, calls=%fused_computation | convolution fusion | flops 4833411072 | bytes 16908288 | tf_op jit(solution)/shard_map/dot_general | solution.py:699
  141.4 0.0 copy-start.6
  141.4 1.6 %copy-done.6 = bf16[384,4096]{1,0:T(8,128)(2,1)} copy-done((bf16[384,4096]{1,0:T(8,128)(2,1)}, bf16[384,4096]{1,0:T(8,128)(2,1)S(1)}, u32[]{:S(2)}) %copy-start.6) | copy-done | bytes 3145752
  143.1 0.0 copy-start.7
  143.1 1.3 constant_dynamic-slice_fusion
  144.4 2.0 %collective-permute-start.1 = (bf16[384,2048]{1,0:T(8,128)(2,1)}, bf16[384,2048]{1,0:T(8,128)(2,1)S(1)}, u32[]{:S(2)}, u32[]{:S(2)}) collective-permute-start(bf16[384,2048]{1,0:T(8,128)(2,1)} %constant_dynamic-slice_fusion), channel_id=1, source_target_pairs={{0,1},{1,0},{2,3},{3,2},{4,5},{5,4},{6,7},{7,6},{8,9},{9,8},{10,11... | collective-permute-start | bytes 4718600 | tf_op jit(solution)/shard_map/ppermute | solution.py:709
  146.4 0.0 copy-done.7
  146.4 3.2 %collective-permute-done.1 = bf16[384,2048]{1,0:T(8,128)(2,1)S(1)} collective-permute-done((bf16[384,2048]{1,0:T(8,128)(2,1)}, bf16[384,2048]{1,0:T(8,128)(2,1)S(1)}, u32[]{:S(2)}, u32[]{:S(2)}) %collective-permute-start.1) | collective-permute-done | bytes 1572896 | tf_op jit(solution)/shard_map/ppermute | solution.py:709
  149.7 2.0 %multiply_reduce_fusion = f32[384]{0:T(512)S(1)} fusion(bf16[384,2048]{1,0:T(8,128)(2,1)S(1)} %collective-permute-done.1, bf16[384,4096]{1,0:T(8,128)(2,1)} %copy-done.6, s32[]{:T(128)S(6)} %select_n.43), kind=kLoop, calls=%fused_computation.2 | loop fusion | flops 3931776 | bytes 3147268 | tf_op jit(solution)/shard_map/reduce_sum | solution.py:710
  151.7 2.5 %psum.7 = f32[384]{0:T(512)S(1)} all-reduce(f32[384]{0:T(512)S(1)} %multiply_reduce_fusion), channel_id=1, replica_groups=mesh['sp'=4,'fs'=4,'tp'=2] {'tp'}, use_global_device_ids=true, to_apply=%region_1.2 | all-reduce | flops 384 | bytes 3072 | tf_op jit(solution)/shard_map/psum | solution.py:710
  154.2 3.4 %fusion = bf16[1,384,2048]{2,1,0:T(8,128)(2,1)} fusion(bf16[384,2048]{1,0:T(8,128)(2,1)S(1)} %collective-permute-done.1, f32[2048]{0:T(1024)S(1)} %dynamic-slice_convert_fusion, f32[384]{0:T(512)S(1)} %add_rsqrt_fusion, bf16[384,4096]{1,0:T(8,128)(2,1)} %copy-done.6, s32[]{:T(128)S(6)} %select_n.43), kind=kLoop, calls=%fused_computation.4 | loop fusion | flops 4718592 | bytes 4728324 | tf_op jit(solution)/shard_map/broadcast_in_dim | solution.py:712
  (9 shorter events, 0.1 us)
Async XLA Ops:
  0.0 10.4 %copy-start = (bf16[4,256,256]{2,1,0:T(8,128)(2,1)S(1)}, bf16[4,256,256]{2,1,0:T(8,128)(2,1)}, u32[]{:S(2)}) copy-start(bf16[4,256,256]{2,1,0:T(8,128)(2,1)} %param.31) | copy-start | bytes 1572868
  0.0 13.6 %copy-start.3 = (bf16[1,384,512]{2,1,0:T(8,128)(2,1)S(1)}, bf16[1,384,512]{2,1,0:T(8,128)(2,1)}, u32[]{:S(2)}) copy-start(bf16[1,384,512]{2,1,0:T(8,128)(2,1)} %param.30) | copy-start | bytes 1179652
  0.0 13.6 %copy-start.1 = (bf16[1,384,1024]{2,1,0:T(8,128)(2,1)S(1)}, bf16[1,384,1024]{2,1,0:T(8,128)(2,1)}, u32[]{:S(2)}) copy-start(bf16[1,384,1024]{2,1,0:T(8,128)(2,1)} %param.18) | copy-start | bytes 2359300
  0.0 13.6 %copy-start.4 = (f32[1,384,16]{1,2,0:T(8,128)S(1)}, f32[1,384,16]{1,2,0:T(8,128)}, u32[]{:S(2)}) copy-start(f32[1,384,16]{1,2,0:T(8,128)} %param.23) | copy-start | bytes 73732
  0.0 13.6 %copy-start.5 = (bf16[1,384,16]{1,2,0:T(8,128)(2,1)S(1)}, bf16[1,384,16]{1,2,0:T(8,128)(2,1)}, u32[]{:S(2)}) copy-start(bf16[1,384,16]{1,2,0:T(8,128)(2,1)} %param.22) | copy-start | bytes 36868
  3.0 9.8 %collective-permute-start = (bf16[15,2048]{1,0:T(8,128)(2,1)}, bf16[15,2048]{1,0:T(8,128)(2,1)}, u32[]{:S(2)}, u32[]{:S(2)}) collective-permute-start(bf16[15,2048]{1,0:T(8,128)(2,1)} %fusion.7), channel_id=1, source_target_pairs={{0,8},{8,16},{16,24},{1,9},{9,17},{17,25},{2,10},{10,18},{18,26},{... | collective-permute-start | bytes 184328 | tf_op jit(solution)/shard_map/ppermute | solution.py:25
  13.6 1.1 copy-start.2
  141.4 1.6 %copy-start.6 = (bf16[384,4096]{1,0:T(8,128)(2,1)}, bf16[384,4096]{1,0:T(8,128)(2,1)S(1)}, u32[]{:S(2)}) copy-start(bf16[384,4096]{1,0:T(8,128)(2,1)S(1)} %convolution_convert_fusion) | copy-start | bytes 9437188
  143.1 3.4 %copy-start.7 = (bf16[4096]{0:T(1024)(128)(2,1)S(1)}, bf16[4096]{0:T(1024)(128)(2,1)}, u32[]{:S(2)}) copy-start(bf16[4096]{0:T(1024)(128)(2,1)} %param.35) | copy-start | bytes 24580
  144.4 5.3 %collective-permute-start.1 = (bf16[384,2048]{1,0:T(8,128)(2,1)}, bf16[384,2048]{1,0:T(8,128)(2,1)S(1)}, u32[]{:S(2)}, u32[]{:S(2)}) collective-permute-start(bf16[384,2048]{1,0:T(8,128)(2,1)} %constant_dynamic-slice_fusion), channel_id=1, source_target_pairs={{0,1},{1,0},{2,3},{3,2},{4,5},{5,4},{6,7},{7,6},{8,9},{9,8},{10,11... | collective-permute-start | bytes 4718600 | tf_op jit(solution)/shard_map/ppermute | solution.py:709
